TPU v7x, 32 devices: a whole 2x2x4 slice. The times are simulated.
32 devices in a mesh: sp: 16 (over z, y, x), tp: 2 (over core).
Axes of the slice: x: 2, y: 2, z: 4, core: 2. Of those that a mesh axis runs over, the one named last changes fastest.
Arguments:
- mid_stream: bfloat16 [5120, 2048], P('sp', 'tp'), may hold values from -6 to 6
- layer_cot: bfloat16 [5120, 2048], P('sp', 'tp'), may hold values from -6 to 6
- ffn_gain: bfloat16 [2048], P('tp'), may hold values from 0.099609375 to 1.8984375
- expert_ids: int32 [5120, 2], P('sp'), may hold values from 0 to 15, all different within a row; in each aligned block of 320 rows (0 to 319, 320 to 639, ...) at most 80 rows name the same one
- group_prob: float32 [5120], P('sp'), may hold values from 0.25 to 1
- first_share: float32 [5120], P('sp'), may hold values from 0.5 to 0.95
- expert_gate: bfloat16 [16, 2048, 1024], P('sp', None, 'tp'), may hold values from -0.125 to 0.125
- expert_up: bfloat16 [16, 2048, 1024], P('sp', None, 'tp'), may hold values from -0.125 to 0.125
- expert_down: bfloat16 [16, 1024, 2048], P('sp', 'tp'), may hold values from -0.1875 to 0.1875
- out_weight: bfloat16 [2048, 1024], P(None, 'tp'), may hold values from -0.1875 to 0.1875
- conv_gain: bfloat16 [1024], P('tp'), may hold values from 0.099609375 to 1.8984375
- b_gate: bfloat16 [5120, 1024], P('sp', 'tp'), may hold values from -6 to 6
- c_gate: bfloat16 [5120, 1024], P('sp', 'tp'), may hold values from -6 to 6
- conv_in: bfloat16 [5120, 1024], P('sp', 'tp'), may hold values from -6 to 6
- conv_out: bfloat16 [5120, 1024], P('sp', 'tp'), may hold values from -6 to 6
- conv_taps: bfloat16 [3, 1024], P(None, 'tp'), may hold values from -3.5 to 3.5
Outputs:
- grad_gate: float32 [16, 2048, 1024], P('sp', None, 'tp')
- grad_up: float32 [16, 2048, 1024], P('sp', None, 'tp')
- grad_down: float32 [16, 1024, 2048], P('sp', 'tp')
- grad_out_weight: float32 [2048, 1024], P('sp', 'tp')
- mid_grad: bfloat16 [5120, 2048], P('sp', 'tp')
- grad_b: bfloat16 [5120, 1024], P('sp', 'tp')
- grad_c: bfloat16 [5120, 1024], P('sp', 'tp')
- grad_conv_in: bfloat16 [5120, 1024], P('sp', 'tp')
Inputs may be any that keep to these rules, and one draw needn't show every extreme that they name: `expert_ids`: each row names 2 different experts. Among the rows of one device no expert is named more than 80 times, a bound that some block reaches.
All inputs are finite; a program needn't handle non-finite values.
Results may differ from a plain program's by a relative error of at most 0.0067.
Values may be sent and summed in bfloat16 or wider, within the bound.
A program may use at most 128 MiB of HBM per device.

v0:
```python
import functools

import jax
import jax.numpy as jnp
from jax import lax
from jax.experimental import pallas as pl
from jax.experimental.pallas import tpu as pltpu
from jax.sharding import PartitionSpec as P

GROUP = 64
MESH = pl.DeviceIdType.MESH
VMEM_LIMIT = 63 * 1024 * 1024
COL = 256

epsilon = 1e-06

f32, bf16 = jnp.float32, jnp.bfloat16


def from_behind(block, axis, distance):
    devices = range(lax.axis_size(axis))
    route = [(i - distance, i) for i in devices if i - distance in devices]
    return lax.ppermute(block, axis, route)


def silu_parts(pre):
    sigma = jax.nn.sigmoid(pre)
    return (pre * sigma, sigma * (1.0 + pre * (1.0 - sigma)))


def contract_rows(left, right):
    return lax.dot_general(
        left, right, (((0,), (0,)), ((), ())), preferred_element_type=jnp.float32
    )


def contract_cols(left, right):
    return lax.dot_general(
        left, right, (((1,), (1,)), ((), ())), preferred_element_type=jnp.float32
    )


def remote(src, dst, send, recv, where):
    return pltpu.make_async_remote_copy(
        src_ref=src,
        dst_ref=dst,
        send_sem=send,
        recv_sem=recv,
        device_id=where,
        device_id_type=MESH,
    )


def cols_at(start, size):
    return pl.ds(pl.multiple_of(start, size), size)


def greet(planes, plane, z, q, c):
    barrier = pltpu.get_barrier_semaphore()
    me = z * plane + q

    def hello(peer, core):
        pl.semaphore_signal(barrier, inc=1, device_id=(peer, core), device_id_type=MESH)

    @pl.loop(1, plane)
    def _(k):
        hello(z * plane + lax.rem(q + k, plane), c)

    hello(me, 1 - c)

    @pl.when(z > 0)
    def _():
        hello(me - plane, c)

    @pl.when(z < planes - 1)
    def _():
        hello(me + plane, c)

    pl.semaphore_wait(barrier, plane + jnp.minimum(z, 1) + jnp.minimum(planes - 1 - z, 1))


def expert_kernel(
    dims,
    mid_in, cot_in, meta_in, gain, gate_in, up_in, down_in,
    mid_grad, full, tokens_out, cots_out, hid_out, dgate_out, dup_out,
    mid_all, cot_all, meta_all, place, share_col, rows_tok, rows_cot, tokens, cots,
    hid, dgate, dup, active, slope, part, theirs, total, back, chain, dn, inner,
    gate, up, down,
    ld, meta_sem, z_up, z_dn, z_recv, p_send, p_recv, f_send, f_recv, own_sem,
    x_send, x_recv, b_send, b_recv, c_send, c_recv, fin, out_sem,
):
    A, B, cap, R, H, F = dims
    S, W = B * cap, 2 * H
    tiles = H // COL
    me, c = lax.axis_index("sp"), lax.axis_index("tp")
    z, q = lax.div(me, B), lax.rem(me, B)
    partner = (me, 1 - c)
    cols = cols_at(c * H, H)
    other = cols_at((1 - c) * H, H)

    def slots_of(source):
        return cols_at(source * cap, cap)

    def group_of(b):
        return cols_at(b * S, S)

    def order(s):
        low = jnp.minimum(z, A - 1 - z)
        step = lax.div(s + 1, 2)
        near = jnp.where(lax.rem(s, 2) == 1, z - step, z + step)
        far = jnp.where(z < A - 1 - z, s, A - 1 - s)
        return jnp.where(s <= 2 * low, near, far)

    down_first = A - 1 - z <= z

    def chain_order(j):
        below = jnp.where(down_first, z - 1 - j, z - 1 - (j - (A - 1 - z)))
        above = jnp.where(down_first, z + 1 + (j - z), z + 1 + j)
        take_below = jnp.where(down_first, j < z, j >= A - 1 - z)
        return jnp.where(take_below, below, above)

    loads = [
        pltpu.make_async_copy(meta_in, meta_all.at[z, c], ld.at[0]),
        pltpu.make_async_copy(mid_in, mid_all.at[z], ld.at[1]),
        pltpu.make_async_copy(cot_in, cot_all.at[z], ld.at[2]),
        pltpu.make_async_copy(gate_in, gate, ld.at[3]),
        pltpu.make_async_copy(up_in, up, ld.at[4]),
        pltpu.make_async_copy(down_in, down, ld.at[5]),
    ]
    for load in loads:
        load.start()

    greet(A, B, z, q, c)

    remote(meta_in, meta_all.at[z, c], meta_sem.at[0], meta_sem.at[1], partner).start()

    stores = (meta_all, mid_all, cot_all)

    def z_copy(a, b, up_way):
        where = (me + B, c) if up_way else (me - B, c)
        sems = z_up if up_way else z_dn
        return remote(stores[a].at[b], stores[a].at[b], sems.at[a, b], z_recv.at[a, b], where)

    def z_both(a):
        @pl.when(z < A - 1)
        def _():
            z_copy(a, z, True).start()

        @pl.when(z > 0)
        def _():
            z_copy(a, z, False).start()

    loads[0].wait()
    remote(meta_in, meta_all.at[z, 1 - c], meta_sem.at[0], meta_sem.at[1], partner).wait()
    z_both(0)
    loads[1].wait()
    z_both(1)
    loads[2].wait()
    z_both(2)

    def arrive(a, b):
        @pl.when(b != z)
        def _():
            remote(
                stores[a].at[b], stores[a].at[b], z_up.at[a, b], z_recv.at[a, b], partner
            ).wait_recv()

            @pl.when((b < z) & (z < A - 1))
            def _():
                z_copy(a, b, True).start()

            @pl.when((b > z) & (z > 0))
            def _():
                z_copy(a, b, False).start()

    rows = (rows_tok, rows_cot)
    inbox = (tokens, cots)

    def plane_send(a, b, k):
        peer = lax.rem(q + k, B)
        return remote(
            rows[a].at[slots_of(peer)],
            inbox[a].at[slots_of(b * B + q), cols],
            p_send.at[a, k],
            p_recv.at[a, b, k],
            (z * B + peer, c),
        )

    def plane_incoming(a, b, k):
        source = lax.rem(q + B - k, B)
        spot = inbox[a].at[slots_of(b * B + source), cols]
        return remote(spot, spot, p_send.at[a, k], p_recv.at[a, b, k], partner)

    def forward(a, b, k):
        source = lax.rem(q + B - k, B)
        spot = inbox[a].at[slots_of(b * B + source), cols]
        return remote(spot, spot, f_send.at[a, b, k], f_recv.at[a, b, k], partner)

    def forwarded(a, b, k):
        source = lax.rem(q + B - k, B)
        spot = inbox[a].at[slots_of(b * B + source), other]
        return remote(spot, spot, f_send.at[a, b, k], f_recv.at[a, b, k], partner)

    def own_local(a, b):
        return pltpu.make_async_copy(
            rows[a].at[slots_of(q)], inbox[a].at[slots_of(b * B + q), cols], own_sem.at[a]
        )

    def own_partner(a, b):
        return remote(
            rows[a].at[slots_of(q)],
            inbox[a].at[slots_of(b * B + q), cols],
            f_send.at[a, b, 0],
            f_recv.at[a, b, 0],
            partner,
        )

    def rows_out(a, b):
        @pl.loop(1, B)
        def _(k):
            plane_send(a, b, k).start()

        own_local(a, b).start()
        own_partner(a, b).start()

    def rows_sent(a, b):
        @pl.loop(1, B)
        def _(k):
            plane_send(a, b, k).wait_send()

        own_local(a, b).wait()
        own_partner(a, b).wait_send()

    def meta_rows(b):
        first, second = meta_all[b, 0], meta_all[b, 1]
        inv = lax.rsqrt((first[4:5] + second[4:5]) / W + epsilon)
        base = lax.convert_element_type(z * S, f32)
        return first[0:1] - base, first[1:2] - base, first[2:3], first[3:4], inv

    def pick_tokens(b):
        slot0, slot1, share0, share1, inv = meta_rows(b)
        slot = lax.broadcasted_iota(jnp.int32, (S, R), 0).astype(f32)
        at0, at1 = slot == slot0, slot == slot1
        hit = at0 | at1
        place[b] = jnp.where(hit, 1.0, 0.0).astype(bf16)
        inv_col = jnp.sum(jnp.where(hit, inv, 0.0), axis=1, keepdims=True)
        share_col[...] = jnp.sum(
            jnp.where(at0, share0, jnp.where(at1, share1, 0.0)), axis=1, keepdims=True
        )

        @pl.loop(0, tiles)
        def _(t):
            tile = cols_at(t * COL, COL)
            picked = jnp.dot(place[b], mid_all[b, :, tile], preferred_element_type=f32)
            rows_tok[:, tile] = (picked * inv_col * gain[:, tile]).astype(bf16)

        rows_out(0, b)

    def pick_cots(b):
        @pl.loop(0, tiles)
        def _(t):
            tile = cols_at(t * COL, COL)
            picked = jnp.dot(place[b], cot_all[b, :, tile], preferred_element_type=f32)
            rows_cot[:, tile] = (picked * share_col[...]).astype(bf16)

        rows_out(1, b)

    def swap(b):
        return remote(
            part.at[:, other], theirs.at[b], x_send.at[b], x_recv.at[b], partner
        )

    def give_back(b, k):
        peer = lax.rem(q + k, B)
        return remote(
            total.at[slots_of(peer)],
            back.at[b, slots_of(q)],
            b_send.at[k],
            b_recv.at[b, k],
            (z * B + peer, c),
        )

    def given_back(b, k):
        spot = back.at[b, slots_of(lax.rem(q + B - k, B))]
        return remote(spot, spot, b_send.at[k], b_recv.at[b, k], partner)

    def outs_of(b):
        pairs = (
            (tokens, tokens_out), (cots, cots_out), (hid, hid_out), (dgate, dgate_out), (dup, dup_out)
        )
        return [
            pltpu.make_async_copy(src.at[group_of(b)], dst.at[group_of(b)], out_sem.at[a, b])
            for a, (src, dst) in enumerate(pairs)
        ]

    def run_experts(i):
        b = order(i)
        here = group_of(b)

        for a in range(2):
            @pl.loop(1, B)
            def _(k):
                plane_incoming(a, b, k).wait_recv()
                forward(a, b, k).start()

        @pl.loop(0, B)
        def _(k):
            forwarded(0, b, k).wait_recv()

        @pl.loop(0, F // COL)
        def _(t):
            tile = cols_at(t * COL, COL)
            pre_gate = jnp.dot(tokens[here, :], gate[:, tile], preferred_element_type=f32)
            pre_up = jnp.dot(tokens[here, :], up[:, tile], preferred_element_type=f32)
            lit, lean = silu_parts(pre_gate)
            hid[here, tile] = (lit * pre_up).astype(bf16)
            active[:, tile] = lit
            slope[:, tile] = pre_up * lean

        @pl.loop(0, B)
        def _(k):
            forwarded(1, b, k).wait_recv()

        @pl.loop(0, F // COL)
        def _(t):
            tile = cols_at(t * COL, COL)
            d_hidden = contract_cols(cots[here, :], down[tile, :])
            dgate[here, tile] = (d_hidden * slope[:, tile]).astype(bf16)
            dup[here, tile] = (d_hidden * active[:, tile]).astype(bf16)

        for copy in outs_of(b):
            copy.start()

        @pl.when(i > 0)
        def _():
            swap(order(i - 1)).wait_send()

        def part_half(core):
            @pl.loop(0, tiles)
            def _(t):
                tile = cols_at(core * H + t * COL, COL)
                got = contract_cols(dgate[here, :], gate[tile, :])
                got = got + contract_cols(dup[here, :], up[tile, :])
                part[:, tile] = got.astype(bf16)

        part_half(1 - c)
        swap(b).start()
        part_half(c)

        @pl.when(i > 0)
        def _():
            @pl.loop(1, B)
            def _(k):
                give_back(order(i - 1), k).wait_send()

        swap(b).wait_recv()

        @pl.loop(1, B + 1)
        def _(k):
            peer = lax.rem(q + k, B)
            total[slots_of(peer), :] = (
                part[slots_of(peer), cols].astype(f32) + theirs[b, slots_of(peer), :].astype(f32)
            ).astype(bf16)

        @pl.loop(1, B)
        def _(k):
            give_back(b, k).start()

        back[b, slots_of(q), :] = total[slots_of(q), :]

    def all_back(b):
        @pl.loop(1, B)
        def _(k):
            given_back(b, k).wait_recv()

    def chain_copy(b, t, up_way):
        tile = cols_at(t * COL, COL)
        if up_way:
            spot = jnp.where(b == z + 1, A, b)
            where = (me + B, c)
        else:
            spot, where = b, (me - B, c)
        return remote(
            chain.at[b, :, tile], chain.at[spot, :, tile], c_send.at[b, t], c_recv.at[spot, t], where
        )

    def chain_arrives(spot, t):
        at = chain.at[spot, :, cols_at(t * COL, COL)]
        remote(at, at, c_send.at[spot, t], c_recv.at[spot, t], partner).wait_recv()

    def pass_on(j):
        b = chain_order(j)
        all_back(b)
        fed = ((b < z) & (z < A - 1)) | ((b > z) & (z > 0))

        @pl.loop(0, tiles)
        def _(t):
            tile = cols_at(t * COL, COL)
            mine = contract_rows(place[b], back[b, :, tile])

            @pl.when(fed)
            def _():
                chain_arrives(b, t)
                chain[b, :, tile] = (mine + chain[b, :, tile].astype(f32)).astype(bf16)

            @pl.when(jnp.logical_not(fed))
            def _():
                chain[b, :, tile] = mine.astype(bf16)

            @pl.when(b < z)
            def _():
                chain_copy(b, t, False).start()

            @pl.when(b > z)
            def _():
                chain_copy(b, t, True).start()

    at_end = (z == 0) | (z == A - 1)

    @pl.loop(0, A)
    def _(i):
        b = order(i)
        arrive(0, b)
        arrive(1, b)

        @pl.when(i > 0)
        def _():
            rows_sent(0, order(i - 1))
            rows_sent(1, order(i - 1))

        pick_tokens(b)

        @pl.when(i == 0)
        def _():
            for load in loads[3:]:
                load.wait()

        @pl.when(i > 0)
        def _():
            run_experts(i - 1)

        arrive(2, b)
        pick_cots(b)

        @pl.when(at_end & (i > 1))
        def _():
            pass_on(i - 2)

    rows_sent(0, order(A - 1))
    rows_sent(1, order(A - 1))
    run_experts(A - 1)

    @pl.loop(0, A - 1)
    def _(j):
        @pl.when(jnp.logical_not(at_end) | (j == A - 2))
        def _():
            pass_on(j)

    all_back(z)
    inner[0] = jnp.zeros((R, 128), f32)

    @pl.loop(0, tiles)
    def _(t):
        tile = cols_at(t * COL, COL)
        dn[:, tile] = contract_rows(place[z], back[z, :, tile])

        @pl.when(z < A - 1)
        def _():
            chain_arrives(z, t)
            dn[:, tile] += chain[z, :, tile].astype(f32)

        @pl.when(z > 0)
        def _():
            chain_arrives(A, t)
            dn[:, tile] += chain[A, :, tile].astype(f32)

        g_dn = gain[:, tile] * dn[:, tile]
        dn[:, tile] = g_dn
        summed = jnp.sum(mid_all[z, :, tile].astype(f32) * g_dn, axis=1, keepdims=True)
        inner[0] += jnp.broadcast_to(summed, (R, 128))

    share_inner = remote(inner.at[0], inner.at[1], fin.at[0], fin.at[1], partner)
    share_inner.start()
    inv = meta_rows(z)[4]
    eye = lax.broadcasted_iota(jnp.int32, (R, R), 0) == lax.broadcasted_iota(jnp.int32, (R, R), 1)
    inv_tok = jnp.sum(jnp.where(eye, inv, 0.0), axis=1, keepdims=True)
    share_inner.wait()
    drop = inv_tok * inv_tok * inv_tok * ((inner[0, :, 0:1] + inner[1, :, 0:1]) / W)

    @pl.loop(0, tiles)
    def _(t):
        tile = cols_at(t * COL, COL)
        turned = (
            cot_all[z, :, tile].astype(f32)
            + inv_tok * dn[:, tile]
            - mid_all[z, :, tile].astype(f32) * drop
        ).astype(bf16)
        mid_grad[:, tile] = turned
        full[:, cols_at(c * H + t * COL, COL)] = turned

    share_mid = remote(full.at[:, cols], full.at[:, cols], fin.at[2], fin.at[3], partner)
    share_mid.start()

    @pl.loop(0, A)
    def _(b):
        for copy in outs_of(b):
            copy.wait()
        for a in range(2):
            @pl.loop(1, B)
            def _(k):
                forward(a, b, k).wait_send()

        for a in range(3):
            @pl.when((b <= z) & (z < A - 1))
            def _():
                z_copy(a, b, True).wait_send()

            @pl.when((b >= z) & (z > 0))
            def _():
                z_copy(a, b, False).wait_send()

        @pl.loop(0, tiles)
        def _(t):
            @pl.when(b < z)
            def _():
                chain_copy(b, t, False).wait_send()

            @pl.when(b > z)
            def _():
                chain_copy(b, t, True).wait_send()

    swap(order(A - 1)).wait_send()

    @pl.loop(1, B)
    def _(k):
        give_back(order(A - 1), k).wait_send()

    share_mid.wait_send()
    remote(full.at[:, other], full.at[:, other], fin.at[2], fin.at[3], partner).wait_recv()


def experts(mid, cot, meta, gain, gate, up, down, n, cap, plane, ident):
    R, H = mid.shape
    F = gate.shape[1]
    W = 2 * H
    B = plane
    A = n // B
    S = B * cap
    anywhere = pl.BlockSpec(memory_space=pl.ANY)
    vmem = pl.BlockSpec(memory_space=pltpu.VMEM)
    dma = pltpu.SemaphoreType.DMA
    tiles = H // COL
    dims = (A, B, cap, R, H, F)
    return pl.pallas_call(
        functools.partial(expert_kernel, dims),
        out_shape=(
            jax.ShapeDtypeStruct((R, H), bf16),
            jax.ShapeDtypeStruct((R, W), bf16),
            jax.ShapeDtypeStruct((A * S, W), bf16),
            jax.ShapeDtypeStruct((A * S, W), bf16),
            jax.ShapeDtypeStruct((A * S, F), bf16),
            jax.ShapeDtypeStruct((A * S, F), bf16),
            jax.ShapeDtypeStruct((A * S, F), bf16),
        ),
        in_specs=[anywhere, anywhere, vmem, vmem, anywhere, anywhere, anywhere],
        out_specs=(vmem, vmem) + (anywhere,) * 5,
        scratch_shapes=[
            pltpu.VMEM((A, R, H), bf16),
            pltpu.VMEM((A, R, H), bf16),
            pltpu.VMEM((A, 2, 8, R), f32),
            pltpu.VMEM((A, S, R), bf16),
            pltpu.VMEM((S, 1), f32),
            pltpu.VMEM((S, H), bf16),
            pltpu.VMEM((S, H), bf16),
            pltpu.VMEM((A * S, W), bf16),
            pltpu.VMEM((A * S, W), bf16),
            pltpu.VMEM((A * S, F), bf16),
            pltpu.VMEM((A * S, F), bf16),
            pltpu.VMEM((A * S, F), bf16),
            pltpu.VMEM((S, F), f32),
            pltpu.VMEM((S, F), f32),
            pltpu.VMEM((S, W), bf16),
            pltpu.VMEM((A, S, H), bf16),
            pltpu.VMEM((S, H), bf16),
            pltpu.VMEM((A, S, H), bf16),
            pltpu.VMEM((A + 1, R, H), bf16),
            pltpu.VMEM((R, H), f32),
            pltpu.VMEM((2, R, 128), f32),
            pltpu.VMEM((W, F), bf16),
            pltpu.VMEM((W, F), bf16),
            pltpu.VMEM((F, W), bf16),
            dma((6,)),
            dma((2,)),
            dma((3, A)),
            dma((3, A)),
            dma((3, A)),
            dma((2, B)),
            dma((2, A, B)),
            dma((2, A, B)),
            dma((2, A, B)),
            dma((2,)),
            dma((A,)),
            dma((A,)),
            dma((B,)),
            dma((A, B)),
            dma((A, tiles)),
            dma((A + 1, tiles)),
            dma((4,)),
            dma((5, A)),
        ],
        compiler_params=pltpu.CompilerParams(
            collective_id=ident, has_side_effects=True, vmem_limit_bytes=VMEM_LIMIT
        ),
        name="experts",
    )(mid, cot, meta, gain, gate, up, down)


def combine_kernel(dims, full, normed, out, term, plane_in, line_out, line_in, p_send, p_recv, l_send, l_recv):
    A, B, rows, F = dims
    me, c = lax.axis_index("sp"), lax.axis_index("tp")
    z, q = lax.div(me, B), lax.rem(me, B)
    barrier = pltpu.get_barrier_semaphore()

    @pl.loop(1, B)
    def _(k):
        pl.semaphore_signal(
            barrier, inc=1, device_id=(z * B + lax.rem(q + k, B), c), device_id_type=MESH
        )

    @pl.loop(1, A)
    def _(j):
        pl.semaphore_signal(
            barrier, inc=1, device_id=(lax.rem(z + j, A) * B + q, c), device_id_type=MESH
        )

    def lot(x):
        return pl.ds(pl.multiple_of(x * rows, rows), rows)

    def plane_send(s, k):
        peer = lax.rem(q + k, B)
        return remote(
            term.at[s, lot(peer)], plane_in.at[s, k], p_send.at[s, k], p_recv.at[s, k],
            (z * B + peer, c),
        )

    def line_send(s):
        return remote(
            line_out.at[s], line_in.at[s], l_send.at[s], l_recv.at[s],
            (lax.rem(z + s, A) * B + q, c),
        )

    def product(s):
        block = cols_at(lax.rem(z + s, A) * (B * rows), B * rows)
        got = contract_rows(full[:, block], normed[...])
        term[s] = got.astype(bf16)

    @pl.loop(0, A)
    def _(j):
        s = A - 1 - j
        product(s)

        @pl.when(j == 0)
        def _():
            pl.semaphore_wait(barrier, A + B - 2)

        @pl.loop(1, B)
        def _(k):
            plane_send(s, k).start()

    def plane_sum(s):
        out[...] = term[s, lot(q), :].astype(f32)

        @pl.loop(1, B)
        def _(k):
            plane_send(s, k).wait_recv()
            out[...] += plane_in[s, k].astype(f32)

    @pl.loop(0, A - 1)
    def _(j):
        s = A - 1 - j
        plane_sum(s)
        line_out[s] = out[...].astype(bf16)
        line_send(s).start()

    plane_sum(0)

    @pl.loop(1, A)
    def _(s):
        line_send(s).wait_recv()
        out[...] += line_in[s].astype(f32)

    @pl.loop(0, A)
    def _(s):
        @pl.loop(1, B)
        def _(k):
            plane_send(s, k).wait_send()

        @pl.when(s > 0)
        def _():
            line_send(s).wait_send()


def combine(full, normed, n, plane, ident):
    R, W = full.shape
    F = normed.shape[1]
    A, B = n // plane, plane
    rows = W // n
    vmem = pl.BlockSpec(memory_space=pltpu.VMEM)
    dma = pltpu.SemaphoreType.DMA
    return pl.pallas_call(
        functools.partial(combine_kernel, (A, B, rows, F)),
        out_shape=jax.ShapeDtypeStruct((rows, F), f32),
        in_specs=[vmem, vmem],
        out_specs=vmem,
        scratch_shapes=[
            pltpu.VMEM((A, B * rows, F), bf16),
            pltpu.VMEM((A, B, rows, F), bf16),
            pltpu.VMEM((A, rows, F), bf16),
            pltpu.VMEM((A, rows, F), bf16),
            dma((A, B)),
            dma((A, B)),
            dma((A,)),
            dma((A,)),
        ],
        compiler_params=pltpu.CompilerParams(
            collective_id=ident, has_side_effects=True, vmem_limit_bytes=VMEM_LIMIT
        ),
        name="combine",
    )(full, normed)


def group_mean(values, blocks):
    return jnp.dot(
        values, blocks, precision=lax.Precision.HIGHEST, preferred_element_type=jnp.float32
    ) * (1.0 / GROUP)


def shards(
    mid_stream,
    layer_cot,
    ffn_gain,
    expert_ids,
    group_prob,
    first_share,
    expert_gate,
    expert_up,
    expert_down,
    out_weight,
    conv_gain,
    b_gate,
    c_gate,
    conv_in,
    conv_out,
    conv_taps,
):
    row_count, half_width = mid_stream.shape
    n = lax.axis_size("sp")
    expert_count = n * expert_gate.shape[0]
    slot_count = 4 * row_count // expert_count
    plane = row_count // slot_count
    cap = -(-slot_count // 16) * 16

    mid32 = mid_stream.astype(f32)
    square_sum = jnp.sum(mid32 * mid32, axis=1)
    experts_row = jnp.arange(expert_count, dtype=jnp.int32)[None, :]
    hot = [expert_ids[:, c : c + 1] == experts_row for c in range(2)]
    both = jnp.concatenate([h.astype(bf16) for h in hot], axis=1)
    row = jnp.arange(row_count, dtype=jnp.int32)
    before = (row[None, :] < row[:, None]).astype(bf16)
    counted = jnp.dot(before, both, preferred_element_type=f32)
    first_total = jnp.sum(hot[0].astype(f32), axis=0, keepdims=True)
    rank0 = jnp.sum(jnp.where(hot[0], counted[:, :expert_count], 0.0), axis=1)
    rank1 = jnp.sum(jnp.where(hot[1], counted[:, expert_count:] + first_total, 0.0), axis=1)
    ids = expert_ids.astype(f32)
    none = jnp.zeros_like(rank0)
    meta = jnp.stack(
        [
            ids[:, 0] * cap + rank0,
            ids[:, 1] * cap + rank1,
            group_prob * first_share,
            group_prob * (1.0 - first_share),
            square_sum,
            none,
            none,
            none,
        ],
        axis=0,
    )
    gain32 = ffn_gain.astype(f32)[None, :]
    gate_w, up_w, down_w = expert_gate[0], expert_up[0], expert_down[0]
    mid_grad, full_mid, tokens_in, cots_in, hidden, d_gate, d_up = experts(
        mid_stream, layer_cot, meta, gain32, gate_w, up_w, down_w, n, cap, plane, 1
    )

    channel_count = b_gate.shape[1]
    b32 = b_gate.astype(f32)
    y32 = conv_out.astype(f32)
    gated = b32 * y32
    lane = jnp.arange(channel_count, dtype=jnp.int32) // GROUP
    blocks = (lane[:, None] == lane[None, :]).astype(f32)
    group_rms = lax.rsqrt(group_mean(gated * gated, blocks) + epsilon)
    cgain = conv_gain.astype(f32)[None, :]
    conv_normed = (gated * group_rms * cgain).astype(bf16)

    grad_out_weight = combine(full_mid, conv_normed, n, plane, 2)

    d_normed_conv = jnp.dot(full_mid, out_weight, preferred_element_type=f32)
    g_dc = cgain * d_normed_conv
    group_inner = group_mean(gated * g_dc, blocks)
    d_gated = group_rms * g_dc - gated * (group_rms**3 * group_inner)
    grad_b = (d_gated * y32).astype(bf16)
    d_conv_out = d_gated * b32
    following = from_behind(d_conv_out[:2], "sp", -1)
    grad_down = contract_rows(hidden, cots_in)[None]
    grad_gate = contract_rows(tokens_in, d_gate)[None]
    grad_up = contract_rows(tokens_in, d_up)[None]
    extended = jnp.concatenate([d_conv_out, following], axis=0)
    taps = conv_taps.astype(f32)
    d_mixed = taps[2] * extended[:-2] + taps[1] * extended[1:-1] + taps[0] * extended[2:]
    grad_c = (d_mixed * conv_in.astype(f32)).astype(bf16)
    grad_conv_in = (d_mixed * c_gate.astype(f32)).astype(bf16)
    return (grad_gate, grad_up, grad_down, grad_out_weight, mid_grad, grad_b, grad_c, grad_conv_in)


def solution(mesh):
    placed = (
        P("sp", "tp"),
        P("sp", "tp"),
        P("tp"),
        P("sp", None),
        P("sp"),
        P("sp"),
        P("sp", None, "tp"),
        P("sp", None, "tp"),
        P("sp", "tp", None),
        P(None, "tp"),
        P("tp"),
        P("sp", "tp"),
        P("sp", "tp"),
        P("sp", "tp"),
        P("sp", "tp"),
        P(None, "tp"),
    )
    return jax.shard_map(
        shards,
        mesh=mesh,
        in_specs=placed,
        out_specs=(
            P("sp", None, "tp"),
            P("sp", None, "tp"),
            P("sp", "tp", None),
            P("sp", "tp"),
            P("sp", "tp"),
            P("sp", "tp"),
            P("sp", "tp"),
            P("sp", "tp"),
        ),
        check_vma=False,
    )
```

profile of v0, /device:TPU:0, one launch (start us, length us, event | category | flops | bytes accessed | tf_op | source)
XLA Modules:
  0.0 232.7 jit_solution(3845253733123013321)
XLA Ops:
  0.6 0.8 slice_reduce_fusion.1
  1.4 0.7 convert_element_type.44
  2.1 0.1 convert_reduce_fusion
  2.2 0.7 subtract_multiply_fusion
  3.0 1.3 multiply_reduce_fusion
  4.3 1.3 broadcast_in_dim.32
  5.5 0.7 convert_element_type.49
  6.2 0.2 fusion.37
  6.4 0.1 fusion.42
  6.5 0.6 stack.21.meta_in
  7.2 167.7 %experts.1 = (bf16[320,1024]{1,0:T(8,128)(2,1)}, bf16[320,2048]{1,0:T(8,128)(2,1)}, bf16[1280,2048]{1,0:T(8,128)(2,1)}, bf16[1280,2048]{1,0:T(8,128)(2,1)}, bf16...) custom-call(bf16[320,1024]{1,0:T(8,128)(2,1)} %mid_in.1, bf16[320,1024]{1,0:T(8,128)(2,1)} %cot_in.1, ...), custom_call_target="tpu_custom_call" | custom-call | tf_op jit(solution)/shard_map/experts/pallas_call | solution.py:554
  174.9 0.0 copy-start.8
  174.9 0.0 copy-start.9
  174.9 0.0 copy-start.7
  174.9 3.0 %convolution_multiply_fusion = f32[320,512]{1,0:T(8,128)S(1)} fusion(bf16[320,2048]{1,0:T(8,128)(2,1)} %get-tuple-element.20.full, bf16[2048,512]{1,0:T(8,128)(2,1)} %param.25, f32[512]{0:T(512)S(1)} %convert_element_type.49), kind=kOutput, calls=%fused_computation.15 | convolution fusion | flops 671252480 | bytes 4065280 | tf_op jit(solution)/shard_map/dot_general | solution.py:807
  177.9 0.0 copy-done.8
  177.9 0.0 copy-done.9
  177.9 0.0 copy-start.5
  177.9 0.9 fusion.22
  178.8 2.0 convert_multiply_fusion.2
  180.8 0.6 slice.54
  181.4 1.5 collective-permute-start
  182.9 0.0 copy-done.7
  182.9 0.0 copy-done.5
  182.9 0.0 copy-start.6
  182.9 0.0 slice-start
  182.9 4.5 %convolution_bitcast_fusion.1 = f32[1,2048,512]{2,1,0:T(8,128)} fusion(bf16[1280,2048]{1,0:T(8,128)(2,1)S(1)} %copy-done.5, bf16[1280,512]{1,0:T(8,128)(2,1)S(1)} %copy-done.7), kind=kOutput, calls=%fused_computation.1 | convolution fusion | flops 2684354560 | bytes 10747904 | tf_op jit(solution)/shard_map/dot_general | solution.py:32
  187.4 0.0 copy-done.6
  187.4 0.0 slice-start.1
  187.4 4.4 %convolution_bitcast_fusion.2 = f32[1,2048,512]{2,1,0:T(8,128)} fusion(bf16[1280,2048]{1,0:T(8,128)(2,1)S(1)} %copy-done.5, bf16[1280,512]{1,0:T(8,128)(2,1)S(1)} %copy-done.6), kind=kOutput, calls=%fused_computation.2 | convolution fusion | flops 2684354560 | bytes 10747904 | tf_op jit(solution)/shard_map/dot_general | solution.py:32
  191.8 0.0 slice-done
  191.8 0.0 slice-done.1
  191.8 0.0 copy-done
  191.8 0.0 copy-start.4
  191.8 4.4 %convolution_bitcast_fusion = f32[1,512,2048]{2,1,0:T(8,128)} fusion(bf16[1280,512]{1,0:T(8,128)(2,1)S(1)} %copy-done, bf16[1280,2048]{1,0:T(8,128)(2,1)S(1)} %bitcast.30), kind=kOutput, calls=%fused_computation | convolution fusion | flops 2684354560 | bytes 10747904 | tf_op jit(solution)/shard_map/dot_general | solution.py:32
  196.3 0.0 copy-done.4
  196.3 0.6 fusion.53
  196.9 31.4 %combine.1 = f32[128,512]{1,0:T(8,128)} custom-call(bf16[320,2048]{1,0:T(8,128)(2,1)} %get-tuple-element.20.full, bf16[320,512]{1,0:T(8,128)(2,1)} %get-tuple-element.30.normed), custom_call_target="tpu_custom_call" | custom-call | tf_op jit(solution)/shard_map/combine/pallas_call | solution.py:710
  228.3 0.0 copy-start.1
  228.3 0.0 copy-start.2
  228.3 0.0 collective-permute-done
  228.3 2.0 multiply_convert_fusion
  230.3 0.0 copy-done.3
  230.3 0.8 multiply_convert_fusion.1
  231.2 0.0 copy-done.1
  231.2 0.7 copy.26
  231.9 0.0 copy-done.2
  231.9 0.8 copy.27
  (11 shorter events, 0.0 us)
Async XLA Ops:
  174.9 3.0 %copy-start.8 = (bf16[320,512]{1,0:T(8,128)(2,1)S(1)}, bf16[320,512]{1,0:T(8,128)(2,1)}, u32[]{:S(2)}) copy-start(bf16[320,512]{1,0:T(8,128)(2,1)} %param.27) | copy-start | bytes 983044
  174.9 3.0 %copy-start.9 = (bf16[320,512]{1,0:T(8,128)(2,1)S(1)}, bf16[320,512]{1,0:T(8,128)(2,1)}, u32[]{:S(2)}) copy-start(bf16[320,512]{1,0:T(8,128)(2,1)} %param.30) | copy-start | bytes 983044
  174.9 7.9 %copy-start.7 = (bf16[1280,512]{1,0:T(8,128)(2,1)S(1)}, bf16[1280,512]{1,0:T(8,128)(2,1)}, u32[]{:S(2)}) copy-start(bf16[1280,512]{1,0:T(8,128)(2,1)} %get-tuple-element.17) | copy-start | bytes 3932164
  177.9 5.0 %copy-start.5 = (bf16[1280,2048]{1,0:T(8,128)(2,1)S(1)}, bf16[1280,2048]{1,0:T(8,128)(2,1)}, u32[]{:S(2)}) copy-start(bf16[1280,2048]{1,0:T(8,128)(2,1)} %get-tuple-element.15) | copy-start | bytes 15728644
  181.4 46.9 %collective-permute-start = (f32[2,512]{1,0:T(2,128)}, f32[2,512]{1,0:T(2,128)}, u32[]{:S(2)}, u32[]{:S(2)}) collective-permute-start(f32[2,512]{1,0:T(2,128)} %slice.54), channel_id=1, source_target_pairs={{2,0},{4,2},{6,4},{8,6},{10,8},{12,10},{14,12},{16,14},{18,16},{20... | collective-permute-start | bytes 12296 | tf_op jit(solution)/shard_map/ppermute | solution.py:23
  182.9 4.5 %copy-start.6 = (bf16[1280,512]{1,0:T(8,128)(2,1)S(1)}, bf16[1280,512]{1,0:T(8,128)(2,1)}, u32[]{:S(2)}) copy-start(bf16[1280,512]{1,0:T(8,128)(2,1)} %get-tuple-element.16) | copy-start | bytes 3932164
  182.9 8.9 %slice-start = ((s8[5242880]{0:T(1024)(128)(4,1)}), s8[4194304]{0:T(1024)(128)(4,1)S(1)}, s32[]{:S(2)}) async-start(s8[5242880]{0:T(1024)(128)(4,1)} %bitcast.29), calls=%async_computation | async-start | bytes 8388608
  187.4 4.5 %slice-start.1 = ((s8[5242880]{0:T(1024)(128)(4,1)}), s8[1048576]{0:T(1024)(128)(4,1)S(1)}, s32[]{:S(2)}) async-start(s8[5242880]{0:T(1024)(128)(4,1)} %bitcast.29), calls=%async_computation.1 | async-start | bytes 2097152
  187.4 4.5 %copy-start = (bf16[1280,512]{1,0:T(8,128)(2,1)S(1)}, bf16[1280,512]{1,0:T(8,128)(2,1)}, u32[]{:S(2)}) copy-start(bf16[1280,512]{1,0:T(8,128)(2,1)} %get-tuple-element.18) | copy-start | bytes 3932164
  191.8 4.4 %copy-start.4 = (bf16[3,512]{1,0:T(4,128)(2,1)S(1)}, bf16[3,512]{1,0:T(4,128)(2,1)}, u32[]{:S(2)}) copy-start(bf16[3,512]{1,0:T(4,128)(2,1)} %param.31) | copy-start | bytes 9220
  196.3 34.1 %copy-start.3 = (bf16[320,512]{1,0:T(8,128)(2,1)S(1)}, bf16[320,512]{1,0:T(8,128)(2,1)}, u32[]{:S(2)}) copy-start(bf16[320,512]{1,0:T(8,128)(2,1)} %param.29) | copy-start | bytes 983044
  228.3 2.9 %copy-start.1 = (f32[128,512]{1,0:T(8,128)S(1)}, f32[128,512]{1,0:T(8,128)}, u32[]{:S(2)}) copy-start(f32[128,512]{1,0:T(8,128)} %combine.1) | copy-start | bytes 786436
  228.3 3.6 %copy-start.2 = (bf16[320,1024]{1,0:T(8,128)(2,1)S(1)}, bf16[320,1024]{1,0:T(8,128)(2,1)}, u32[]{:S(2)}) copy-start(bf16[320,1024]{1,0:T(8,128)(2,1)} %get-tuple-element.52) | copy-start | bytes 1966084
where the time goes:
time: 233 us
  Pallas kernels  199 us (85%)
  matrix products  19.3 us (8%)
  other arithmetic  7.79 us (3%)
  local copies, waits for them, and re-layouts  4.21 us (2%)
    pallas_call x1, Pallas kernels, experts(): pl.pallas_call(functools.partial(expert_kernel, dims), out_shape=(jax.Sha...  168 us
    pallas_call x1, Pallas kernels, combine(): pl.pallas_call(functools.partial(combine_kernel, (A, B, rows, F)), out_sh...  31.4 us
    dot_general x3, matrix products, contract_rows(): lax.dot_general(left, right, (((0,), (0,)), ((), ())), preferred_element_...  13.3 us
  transfers between devices with their start and end apart: 1, of which 0 were waited for; matrix products, arithmetic and copies ran while one was open for 6% of the time, Pallas kernels for 13%

commit v1 on v0

v1 whole, which is shorter than its diff:
```python
import functools

import jax
import jax.numpy as jnp
from jax import lax
from jax.experimental import pallas as pl
from jax.experimental.pallas import tpu as pltpu
from jax.sharding import PartitionSpec as P

GROUP = 64
MESH = pl.DeviceIdType.MESH
VMEM_LIMIT = 63 * 1024 * 1024
COL = 256
HALVES = 2

epsilon = 1e-06

f32, bf16 = jnp.float32, jnp.bfloat16


def from_behind(block, axis, distance):
    devices = range(lax.axis_size(axis))
    route = [(i - distance, i) for i in devices if i - distance in devices]
    return lax.ppermute(block, axis, route)


def silu_parts(pre):
    sigma = jax.nn.sigmoid(pre)
    return (pre * sigma, sigma * (1.0 + pre * (1.0 - sigma)))


def contract_rows(left, right):
    return lax.dot_general(
        left, right, (((0,), (0,)), ((), ())), preferred_element_type=jnp.float32
    )


def contract_cols(left, right):
    return lax.dot_general(
        left, right, (((1,), (1,)), ((), ())), preferred_element_type=jnp.float32
    )


def remote(src, dst, send, recv, where):
    return pltpu.make_async_remote_copy(
        src_ref=src,
        dst_ref=dst,
        send_sem=send,
        recv_sem=recv,
        device_id=where,
        device_id_type=MESH,
    )


def cols_at(start, size):
    return pl.ds(pl.multiple_of(start, size), size)


def greet(planes, plane, z, q, c):
    barrier = pltpu.get_barrier_semaphore()
    me = z * plane + q

    def hello(peer, core):
        pl.semaphore_signal(barrier, inc=1, device_id=(peer, core), device_id_type=MESH)

    @pl.loop(1, plane)
    def _(k):
        hello(z * plane + lax.rem(q + k, plane), c)

    hello(me, 1 - c)

    @pl.when(z > 0)
    def _():
        hello(me - plane, c)

    @pl.when(z < planes - 1)
    def _():
        hello(me + plane, c)

    pl.semaphore_wait(barrier, plane + jnp.minimum(z, 1) + jnp.minimum(planes - 1 - z, 1))


def expert_kernel(
    dims,
    mid_in, cot_in, ids, group_prob, first_share, gain_in, gate_in, up_in, down_in,
    mid_grad, full, tokens_out, cots_out, hid_out, dgate_out, dup_out,
    mid_all, cot_all, meta_all, place, inv_col, share_col, rows_tok, rows_cot, tokens, cots,
    hid, dgate, dup, active, slope, part, theirs, total, back, chain, dn, inner, gain,
    gate, up, down,
    ld, meta_sem, z_up, z_dn, z_recv, p_send, p_recv, f_send, f_recv, own_sem,
    x_send, x_recv, b_send, b_recv, c_send, c_recv, fin, out_sem,
):
    A, B, cap, R, H, F = dims
    S, W = B * cap, 2 * H
    tiles = H // COL
    me, c = lax.axis_index("sp"), lax.axis_index("tp")
    z, q = lax.div(me, B), lax.rem(me, B)
    partner = (me, 1 - c)
    cols = cols_at(c * H, H)
    other = cols_at((1 - c) * H, H)

    def slots_of(source):
        return cols_at(source * cap, cap)

    def group_of(b):
        return cols_at(b * S, S)

    above_count = A - 1 - z

    def from_below(r):
        tok = r <= z
        return (r >= 1) & (r <= 2 * z), tok, jnp.where(tok, z - r, r - z - 1)

    def from_above(r):
        tok = r <= above_count
        valid = (r >= 1) & (r <= 2 * above_count)
        return valid, tok, jnp.where(tok, z + r, A + above_count - r)

    sides = (from_below, from_above)

    loads = [
        pltpu.make_async_copy(mid_in, mid_all.at[z], ld.at[0]),
        pltpu.make_async_copy(cot_in, cot_all.at[z], ld.at[1]),
        pltpu.make_async_copy(gate_in, gate, ld.at[2]),
        pltpu.make_async_copy(up_in, up, ld.at[3]),
        pltpu.make_async_copy(down_in, down, ld.at[4]),
    ]
    for load in loads:
        load.start()

    greet(A, B, z, q, c)

    def note_slots():
        crowd = A * B
        row = lax.broadcasted_iota(jnp.int32, (R, R), 0)
        col = lax.broadcasted_iota(jnp.int32, (R, R), 1)
        before = jnp.where(row < col, 1.0, 0.0).astype(bf16)
        expert = lax.broadcasted_iota(jnp.int32, (crowd, R), 0)
        hot = [jnp.where(ids[k : k + 1, :] == expert, 1.0, 0.0) for k in range(2)]
        counted = [jnp.dot(h.astype(bf16), before, preferred_element_type=f32) for h in hot]
        counted[1] = counted[1] + jnp.sum(hot[0], axis=1, keepdims=True)
        squares = jnp.zeros((R, 1), f32)
        for t in range(tiles):
            own = mid_all[z, :, t * COL : (t + 1) * COL].astype(f32)
            squares = squares + jnp.sum(own * own, axis=1, keepdims=True)

        for k in range(2):
            rank = jnp.sum(hot[k] * counted[k], axis=0, keepdims=True)
            meta_all[z, c, k : k + 1, :] = ids[k : k + 1, :].astype(f32) * cap + rank
        prob, first = group_prob[...].reshape(1, R), first_share[...].reshape(1, R)
        meta_all[z, c, 2:3, :] = prob * first
        meta_all[z, c, 3:4, :] = prob * (1.0 - first)
        meta_all[z, c, 4:5, :] = jnp.sum(jnp.where(row == col, squares, 0.0), axis=0, keepdims=True)
        meta_all[z, c, 5:8, :] = jnp.zeros((3, R), f32)
        gain[...] = gain_in[...].astype(f32).reshape(1, H)
        mine = meta_all.at[z, c]
        remote(mine, mine, meta_sem.at[0], meta_sem.at[1], partner).start()
        theirs_at = meta_all.at[z, 1 - c]
        remote(theirs_at, theirs_at, meta_sem.at[0], meta_sem.at[1], partner).wait()

    wide = H // HALVES
    stores = (mid_all, cot_all)

    def piece(h):
        return cols_at(h * wide, wide)

    def z_spot(a, h, b):
        return meta_all.at[b] if a == 2 else stores[a].at[b, :, piece(h)]

    def z_copy(a, h, b, up_way):
        where = (me + B, c) if up_way else (me - B, c)
        sems = z_up if up_way else z_dn
        spot = z_spot(a, h, b)
        return remote(spot, spot, sems.at[a, b], z_recv.at[a, h, b], where)

    def z_own(a, h):
        @pl.when(z < A - 1)
        def _():
            z_copy(a, h, z, True).start()

        @pl.when(z > 0)
        def _():
            z_copy(a, h, z, False).start()

    loads[0].wait()
    for h in range(HALVES):
        z_own(0, h)
    note_slots()
    z_own(2, 0)
    loads[1].wait()

    @pl.when(z == 0)
    def _():
        for h in range(HALVES):
            z_copy(1, h, z, True).start()

    @pl.when(z == A - 1)
    def _():
        for h in range(HALVES):
            z_copy(1, h, z, False).start()

    def landed(a, h, b):
        at = z_spot(a, h, b)
        remote(at, at, z_up.at[a, b], z_recv.at[a, h, b], partner).wait_recv()

    def arrive(r, h):
        for up_way, side in ((True, from_below), (False, from_above)):
            valid, tok, b = side(r)
            onward = (z < A - 1) if up_way else (z > 0)
            last = r == (2 * z if up_way else 2 * above_count)

            @pl.when(valid & tok)
            def _():
                landed(0, h, b)

                @pl.when(onward)
                def _():
                    z_copy(0, h, b, up_way).start()

            @pl.when(valid & tok & (h == HALVES - 1))
            def _():
                landed(2, 0, b)

                @pl.when(onward)
                def _():
                    z_copy(2, 0, b, up_way).start()

            @pl.when(valid & jnp.logical_not(tok))
            def _():
                landed(1, h, b)

                @pl.when(onward)
                def _():
                    z_copy(1, h, b, up_way).start()

            @pl.when(valid & last & onward & (h == HALVES - 1))
            def _():
                for own_h in range(HALVES):
                    z_copy(1, own_h, z, up_way).start()

    rows = (rows_tok, rows_cot)
    inbox = (tokens, cots)

    def in_half(core, h):
        return cols_at(core * H + h * wide, wide)

    def plane_send(a, h, b, k):
        peer = lax.rem(q + k, B)
        return remote(
            rows[a].at[b, slots_of(peer), piece(h)],
            inbox[a].at[slots_of(b * B + q), in_half(c, h)],
            p_send.at[a],
            p_recv.at[a, h, b],
            (z * B + peer, c),
        )

    def plane_landed(a, h, b):
        spot = rows[a].at[b, pl.ds(0, (B - 1) * cap), piece(h)]
        remote(spot, spot, p_send.at[a], p_recv.at[a, h, b], partner).wait_recv()

    def own_local(a, h, b):
        return pltpu.make_async_copy(
            rows[a].at[b, slots_of(q), piece(h)],
            inbox[a].at[slots_of(b * B + q), in_half(c, h)],
            own_sem.at[a, h, b],
        )

    def forward(a, h, b):
        spot = inbox[a].at[group_of(b), in_half(c, h)]
        return remote(spot, spot, f_send.at[a], f_recv.at[a, b], partner)

    def rows_out(a, h, b):
        @pl.loop(1, B)
        def _(k):
            plane_send(a, h, b, k).start()

        own_local(a, h, b).start()

    def meta_rows(b):
        first, second = meta_all[b, 0], meta_all[b, 1]
        inv = lax.rsqrt((first[4:5] + second[4:5]) / W + epsilon)
        base = lax.convert_element_type(z * S, f32)
        return first[0:1] - base, first[1:2] - base, first[2:3], first[3:4], inv

    def find_slots(b):
        slot0, slot1, share0, share1, inv = meta_rows(b)
        slot = lax.broadcasted_iota(jnp.int32, (S, R), 0).astype(f32)
        at0, at1 = slot == slot0, slot == slot1
        hit = at0 | at1
        place[b] = jnp.where(hit, 1.0, 0.0).astype(bf16)
        inv_col[b] = jnp.sum(jnp.where(hit, inv, 0.0), axis=1, keepdims=True)
        share_col[b] = jnp.sum(
            jnp.where(at0, share0, jnp.where(at1, share1, 0.0)), axis=1, keepdims=True
        )

    def pick(a, h, b):
        @pl.loop(0, wide // COL)
        def _(t):
            tile = cols_at(h * wide + t * COL, COL)
            picked = jnp.dot(place[b], stores[a][b, :, tile], preferred_element_type=f32)
            if a == 0:
                rows_tok[b, :, tile] = (picked * inv_col[b] * gain[:, tile]).astype(bf16)
            else:
                rows_cot[b, :, tile] = (picked * share_col[b]).astype(bf16)

        rows_out(a, h, b)

    def swap(b, t):
        tile = cols_at(t * COL, COL)
        return remote(
            part.at[:, cols_at((1 - c) * H + t * COL, COL)],
            theirs.at[b, :, tile],
            x_send.at[t],
            x_recv.at[b, t],
            partner,
        )

    def give_back(b, k, t):
        peer = lax.rem(q + k, B)
        tile = cols_at(t * COL, COL)
        return remote(
            total.at[slots_of(peer), tile],
            back.at[b, slots_of(q), tile],
            b_send.at[t],
            b_recv.at[b, t],
            (z * B + peer, c),
        )

    def given_to(b, t):
        spot = back.at[b, pl.ds(0, (B - 1) * cap), cols_at(t * COL, COL)]
        return remote(spot, spot, b_send.at[t], b_recv.at[b, t], partner)

    def outs_of(b):
        pairs = (
            (tokens, tokens_out), (cots, cots_out), (hid, hid_out), (dgate, dgate_out), (dup, dup_out)
        )
        return [
            pltpu.make_async_copy(src.at[group_of(b)], dst.at[group_of(b)], out_sem.at[a])
            for a, (src, dst) in enumerate(pairs)
        ]

    def take_in(a, b):
        for h in range(HALVES):
            plane_landed(a, h, b)
            own_local(a, h, b).wait()
            forward(a, h, b).start()

    def taken_in(a, b):
        spot = inbox[a].at[group_of(b), other]
        remote(spot, spot, f_send.at[a], f_recv.at[a, b], partner).wait_recv()

    def run_forward(b):
        here = group_of(b)
        taken_in(0, b)

        @pl.loop(0, F // COL)
        def _(t):
            tile = cols_at(t * COL, COL)
            pre_gate = jnp.dot(tokens[here, :], gate[:, tile], preferred_element_type=f32)
            pre_up = jnp.dot(tokens[here, :], up[:, tile], preferred_element_type=f32)
            lit, lean = silu_parts(pre_gate)
            hid[here, tile] = (lit * pre_up).astype(bf16)
            active[here, tile] = lit
            slope[here, tile] = pre_up * lean

    def run_backward(b, before):
        here = group_of(b)
        taken_in(1, b)

        @pl.loop(0, F // COL)
        def _(t):
            tile = cols_at(t * COL, COL)
            d_hidden = contract_cols(cots[here, :], down[tile, :])
            dgate[here, tile] = (d_hidden * slope[here, tile]).astype(bf16)
            dup[here, tile] = (d_hidden * active[here, tile]).astype(bf16)

        for copy in outs_of(b):
            copy.start()

        def part_tile(core, t):
            tile = cols_at(core * H + t * COL, COL)
            got = contract_cols(dgate[here, :], gate[tile, :])
            got = got + contract_cols(dup[here, :], up[tile, :])
            part[:, tile] = got.astype(bf16)

        @pl.loop(0, tiles)
        def _(t):
            @pl.when(before >= 0)
            def _():
                swap(before, t).wait_send()

            part_tile(1 - c, t)
            swap(b, t).start()

        @pl.loop(0, tiles)
        def _(t):
            part_tile(c, t)

            @pl.when(before >= 0)
            def _():
                given_to(b, t).wait_send()

            swap(b, t).wait_recv()
            tile = cols_at(t * COL, COL)
            total[:, tile] = (
                part[:, cols_at(c * H + t * COL, COL)].astype(f32) + theirs[b, :, tile].astype(f32)
            ).astype(bf16)

            @pl.loop(1, B)
            def _(k):
                give_back(b, k, t).start()

            back[b, slots_of(q), tile] = total[slots_of(q), tile]

    def all_back(b, t):
        given_to(b, t).wait_recv()

    def chain_copy(b, t, up_way):
        tile = cols_at(t * COL, COL)
        if up_way:
            spot = jnp.where(b == z + 1, A, b)
            where = (me + B, c)
        else:
            spot, where = b, (me - B, c)
        return remote(
            chain.at[b, :, tile], chain.at[spot, :, tile], c_send, c_recv.at[spot, t], where
        )

    def chain_arrives(spot, t):
        at = chain.at[spot, :, cols_at(t * COL, COL)]
        remote(at, at, c_send, c_recv.at[spot, t], partner).wait_recv()

    def pass_tile(b, t, up_way):
        tile = cols_at(t * COL, COL)
        all_back(b, t)
        mine = contract_rows(place[b], back[b, :, tile])
        fed = (z > 0) if up_way else (z < A - 1)

        @pl.when(fed)
        def _():
            chain_arrives(b, t)
            chain[b, :, tile] = (mine + chain[b, :, tile].astype(f32)).astype(bf16)

        @pl.when(jnp.logical_not(fed))
        def _():
            chain[b, :, tile] = mine.astype(bf16)

        chain_copy(b, t, up_way).start()

    def pass_on(b, up_way):
        @pl.loop(0, tiles)
        def _(t):
            pass_tile(b, t, up_way)

    def settle():
        pairs = ((tokens, tokens_out), (cots, cots_out), (hid, hid_out), (dgate, dgate_out), (dup, dup_out))
        for a, (src, dst) in enumerate(pairs):
            pltpu.make_async_copy(src, dst, out_sem.at[a]).wait()
        for a in range(2):
            sent = rows[a].at[:, pl.ds(0, (B - 1) * cap), :]
            remote(sent, sent, p_send.at[a], p_recv.at[a, 0, 0], partner).wait_send()
            sent = inbox[a].at[:, cols]
            remote(sent, sent, f_send.at[a], f_recv.at[a, 0], partner).wait_send()

        @pl.loop(0, A)
        def _(b):
            for a in range(3):
                whole = meta_all.at[b] if a == 2 else stores[a].at[b]

                @pl.when((b <= z) & (z < A - 1))
                def _():
                    remote(whole, whole, z_up.at[a, b], z_recv.at[a, 0, b], partner).wait_send()

                @pl.when((b >= z) & (z > 0))
                def _():
                    remote(whole, whole, z_dn.at[a, b], z_recv.at[a, 0, b], partner).wait_send()

    at_end = (z == 0) | (z == A - 1)

    find_slots(z)
    for a in range(2):
        for h in range(HALVES):
            pick(a, h, z)
    for load in loads[2:]:
        load.wait()

    def receive(r, h):
        arrive(r, h)

        for side in sides:
            valid, tok, b = side(r)

            @pl.when(valid & tok & (h == HALVES - 1))
            def _():
                find_slots(b)
                for piece_h in range(HALVES):
                    pick(0, piece_h, b)

            @pl.when(valid & jnp.logical_not(tok))
            def _():
                pick(1, h, b)

    run_step = jnp.where(at_end, 0, HALVES - 1)
    lag = jnp.where(at_end, 1, 2)

    def step_of(u, before):
        r, h = lax.div(u, HALVES), lax.rem(u, HALVES)
        receive(r, h)

        @pl.when((r == 1) & (h == 0))
        def _():
            take_in(0, z)
            run_forward(z)

        @pl.when((r == 2) & (h == HALVES - 1 - run_step))
        def _():
            take_in(1, z)
            run_backward(z, -1)

        for side in sides:
            valid, tok, b = side(r - lag)
            now = valid & (h == run_step)

            @pl.when(now & tok)
            def _():
                take_in(0, b)
                run_forward(b)

            @pl.when(now & jnp.logical_not(tok))
            def _():
                take_in(1, b)

        for side in sides:
            valid, tok, b = side(r - lag)
            now = valid & jnp.logical_not(tok) & (h == run_step)

            @pl.when(now)
            def _():
                run_backward(b, before)

            before = jnp.where(now, b, before)

        for up_way, side in ((False, from_below), (True, from_above)):
            valid, tok, b = side(r - 1)

            @pl.when(at_end & valid & jnp.logical_not(tok) & (h == HALVES - 1))
            def _():
                pass_on(b, up_way)

        return before

    last = lax.fori_loop(HALVES, 2 * A * HALVES, step_of, z)

    settle()

    @pl.when(jnp.logical_not(at_end))
    def _():
        @pl.loop(0, A - 1)
        def _(m):
            @pl.loop(0, tiles)
            def _(t):
                @pl.when((above_count <= z) & (m < z))
                def _():
                    pass_tile(m, t, False)

                @pl.when(A - 1 - m > z)
                def _():
                    pass_tile(A - 1 - m, t, True)

                @pl.when((above_count > z) & (m < z))
                def _():
                    pass_tile(m, t, False)

    inner[0] = jnp.zeros((R, 128), f32)

    @pl.loop(0, tiles)
    def _(t):
        tile = cols_at(t * COL, COL)
        all_back(z, t)
        dn[:, tile] = contract_rows(place[z], back[z, :, tile])

        @pl.when(z < A - 1)
        def _():
            chain_arrives(z, t)
            dn[:, tile] += chain[z, :, tile].astype(f32)

        @pl.when(z > 0)
        def _():
            chain_arrives(A, t)
            dn[:, tile] += chain[A, :, tile].astype(f32)

        g_dn = gain[:, tile] * dn[:, tile]
        dn[:, tile] = g_dn
        summed = jnp.sum(mid_all[z, :, tile].astype(f32) * g_dn, axis=1, keepdims=True)
        inner[0] += jnp.broadcast_to(summed, (R, 128))

    share_inner = remote(inner.at[0], inner.at[1], fin.at[0], fin.at[1], partner)
    share_inner.start()
    inv = meta_rows(z)[4]
    eye = lax.broadcasted_iota(jnp.int32, (R, R), 0) == lax.broadcasted_iota(jnp.int32, (R, R), 1)
    inv_tok = jnp.sum(jnp.where(eye, inv, 0.0), axis=1, keepdims=True)
    share_inner.wait()
    drop = inv_tok * inv_tok * inv_tok * ((inner[0, :, 0:1] + inner[1, :, 0:1]) / W)

    @pl.loop(0, tiles)
    def _(t):
        tile = cols_at(t * COL, COL)
        turned = (
            cot_all[z, :, tile].astype(f32)
            + inv_tok * dn[:, tile]
            - mid_all[z, :, tile].astype(f32) * drop
        ).astype(bf16)
        mid_grad[:, tile] = turned
        full[:, cols_at(c * H + t * COL, COL)] = turned

    share_mid = remote(full.at[:, cols], full.at[:, cols], fin.at[2], fin.at[3], partner)
    share_mid.start()

    passed = chain.at[pl.ds(0, A - 1)]
    remote(passed, passed, c_send, c_recv.at[0, 0], partner).wait_send()

    @pl.loop(0, tiles)
    def _(t):
        swap(last, t).wait_send()
        given_to(last, t).wait_send()

    share_mid.wait_send()
    remote(full.at[:, other], full.at[:, other], fin.at[2], fin.at[3], partner).wait_recv()


def experts(mid, cot, ids, prob, first, gain, gate, up, down, n, cap, plane, ident):
    R, H = mid.shape
    F = gate.shape[1]
    W = 2 * H
    B = plane
    A = n // B
    S = B * cap
    anywhere = pl.BlockSpec(memory_space=pl.ANY)
    vmem = pl.BlockSpec(memory_space=pltpu.VMEM)
    dma = pltpu.SemaphoreType.DMA
    tiles = H // COL
    dims = (A, B, cap, R, H, F)
    return pl.pallas_call(
        functools.partial(expert_kernel, dims),
        out_shape=(
            jax.ShapeDtypeStruct((R, H), bf16),
            jax.ShapeDtypeStruct((R, W), bf16),
            jax.ShapeDtypeStruct((A * S, W), bf16),
            jax.ShapeDtypeStruct((A * S, W), bf16),
            jax.ShapeDtypeStruct((A * S, F), bf16),
            jax.ShapeDtypeStruct((A * S, F), bf16),
            jax.ShapeDtypeStruct((A * S, F), bf16),
        ),
        in_specs=[anywhere] * 2 + [vmem] * 4 + [anywhere] * 3,
        out_specs=(vmem, vmem) + (anywhere,) * 5,
        scratch_shapes=[
            pltpu.VMEM((A, R, H), bf16),
            pltpu.VMEM((A, R, H), bf16),
            pltpu.VMEM((A, 2, 8, R), f32),
            pltpu.VMEM((A, S, R), bf16),
            pltpu.VMEM((A, S, 1), f32),
            pltpu.VMEM((A, S, 1), f32),
            pltpu.VMEM((A, S, H), bf16),
            pltpu.VMEM((A, S, H), bf16),
            pltpu.VMEM((A * S, W), bf16),
            pltpu.VMEM((A * S, W), bf16),
            pltpu.VMEM((A * S, F), bf16),
            pltpu.VMEM((A * S, F), bf16),
            pltpu.VMEM((A * S, F), bf16),
            pltpu.VMEM((A * S, F), f32),
            pltpu.VMEM((A * S, F), f32),
            pltpu.VMEM((S, W), bf16),
            pltpu.VMEM((A, S, H), bf16),
            pltpu.VMEM((S, H), bf16),
            pltpu.VMEM((A, S, H), bf16),
            pltpu.VMEM((A + 1, R, H), bf16),
            pltpu.VMEM((R, H), f32),
            pltpu.VMEM((2, R, 128), f32),
            pltpu.VMEM((1, H), f32),
            pltpu.VMEM((W, F), bf16),
            pltpu.VMEM((W, F), bf16),
            pltpu.VMEM((F, W), bf16),
            dma((5,)),
            dma((2,)),
            dma((3, A)),
            dma((3, A)),
            dma((3, HALVES, A)),
            dma((2,)),
            dma((2, HALVES, A)),
            dma((2,)),
            dma((2, A)),
            dma((2, HALVES, A)),
            dma((tiles,)),
            dma((A, tiles)),
            dma((tiles,)),
            dma((A, tiles)),
            dma,
            dma((A + 1, tiles)),
            dma((4,)),
            dma((5,)),
        ],
        compiler_params=pltpu.CompilerParams(
            collective_id=ident, has_side_effects=True, vmem_limit_bytes=VMEM_LIMIT
        ),
        name="experts",
    )(mid, cot, ids, prob, first, gain, gate, up, down)


def combine_kernel(dims, full, normed, out, term, plane_in, line_out, line_in, p_send, p_recv, l_send, l_recv):
    A, B, rows, F = dims
    me, c = lax.axis_index("sp"), lax.axis_index("tp")
    z, q = lax.div(me, B), lax.rem(me, B)
    barrier = pltpu.get_barrier_semaphore()

    @pl.loop(1, B)
    def _(k):
        pl.semaphore_signal(
            barrier, inc=1, device_id=(z * B + lax.rem(q + k, B), c), device_id_type=MESH
        )

    @pl.loop(1, A)
    def _(j):
        pl.semaphore_signal(
            barrier, inc=1, device_id=(lax.rem(z + j, A) * B + q, c), device_id_type=MESH
        )

    def lot(x):
        return pl.ds(pl.multiple_of(x * rows, rows), rows)

    def plane_send(s, k):
        peer = lax.rem(q + k, B)
        return remote(
            term.at[s, lot(peer)], plane_in.at[s, k], p_send.at[s, k], p_recv.at[s, k],
            (z * B + peer, c),
        )

    def line_send(s):
        return remote(
            line_out.at[s], line_in.at[s], l_send.at[s], l_recv.at[s],
            (lax.rem(z + s, A) * B + q, c),
        )

    def product(s):
        block = cols_at(lax.rem(z + s, A) * (B * rows), B * rows)
        got = contract_rows(full[:, block], normed[...])
        term[s] = got.astype(bf16)

    @pl.loop(0, A)
    def _(j):
        s = A - 1 - j
        product(s)

        @pl.when(j == 0)
        def _():
            pl.semaphore_wait(barrier, A + B - 2)

        @pl.loop(1, B)
        def _(k):
            plane_send(s, k).start()

    def plane_sum(s):
        out[...] = term[s, lot(q), :].astype(f32)

        @pl.loop(1, B)
        def _(k):
            plane_send(s, k).wait_recv()
            out[...] += plane_in[s, k].astype(f32)

    @pl.loop(0, A - 1)
    def _(j):
        s = A - 1 - j
        plane_sum(s)
        line_out[s] = out[...].astype(bf16)
        line_send(s).start()

    plane_sum(0)

    @pl.loop(1, A)
    def _(s):
        line_send(s).wait_recv()
        out[...] += line_in[s].astype(f32)

    @pl.loop(0, A)
    def _(s):
        @pl.loop(1, B)
        def _(k):
            plane_send(s, k).wait_send()

        @pl.when(s > 0)
        def _():
            line_send(s).wait_send()


def combine(full, normed, n, plane, ident):
    R, W = full.shape
    F = normed.shape[1]
    A, B = n // plane, plane
    rows = W // n
    vmem = pl.BlockSpec(memory_space=pltpu.VMEM)
    dma = pltpu.SemaphoreType.DMA
    return pl.pallas_call(
        functools.partial(combine_kernel, (A, B, rows, F)),
        out_shape=jax.ShapeDtypeStruct((rows, F), f32),
        in_specs=[vmem, vmem],
        out_specs=vmem,
        scratch_shapes=[
            pltpu.VMEM((A, B * rows, F), bf16),
            pltpu.VMEM((A, B, rows, F), bf16),
            pltpu.VMEM((A, rows, F), bf16),
            pltpu.VMEM((A, rows, F), bf16),
            dma((A, B)),
            dma((A, B)),
            dma((A,)),
            dma((A,)),
        ],
        compiler_params=pltpu.CompilerParams(
            collective_id=ident, has_side_effects=True, vmem_limit_bytes=VMEM_LIMIT
        ),
        name="combine",
    )(full, normed)


def group_mean(values, blocks):
    return jnp.dot(
        values, blocks, precision=lax.Precision.HIGHEST, preferred_element_type=jnp.float32
    ) * (1.0 / GROUP)


def shards(
    mid_stream,
    layer_cot,
    ffn_gain,
    expert_ids,
    group_prob,
    first_share,
    expert_gate,
    expert_up,
    expert_down,
    out_weight,
    conv_gain,
    b_gate,
    c_gate,
    conv_in,
    conv_out,
    conv_taps,
):
    row_count, half_width = mid_stream.shape
    n = lax.axis_size("sp")
    expert_count = n * expert_gate.shape[0]
    slot_count = 4 * row_count // expert_count
    plane = row_count // slot_count
    cap = -(-slot_count // 8) * 8

    gate_w, up_w, down_w = expert_gate[0], expert_up[0], expert_down[0]
    mid_grad, full_mid, tokens_in, cots_in, hidden, d_gate, d_up = experts(
        mid_stream,
        layer_cot,
        expert_ids.T,
        group_prob,
        first_share,
        ffn_gain,
        gate_w,
        up_w,
        down_w,
        n,
        cap,
        plane,
        1,
    )

    channel_count = b_gate.shape[1]
    b32 = b_gate.astype(f32)
    y32 = conv_out.astype(f32)
    gated = b32 * y32
    lane = jnp.arange(channel_count, dtype=jnp.int32) // GROUP
    blocks = (lane[:, None] == lane[None, :]).astype(f32)
    group_rms = lax.rsqrt(group_mean(gated * gated, blocks) + epsilon)
    cgain = conv_gain.astype(f32)[None, :]
    conv_normed = (gated * group_rms * cgain).astype(bf16)

    grad_out_weight = combine(full_mid, conv_normed, n, plane, 2)

    d_normed_conv = jnp.dot(full_mid, out_weight, preferred_element_type=f32)
    g_dc = cgain * d_normed_conv
    group_inner = group_mean(gated * g_dc, blocks)
    d_gated = group_rms * g_dc - gated * (group_rms**3 * group_inner)
    grad_b = (d_gated * y32).astype(bf16)
    d_conv_out = d_gated * b32
    following = from_behind(d_conv_out[:2], "sp", -1)
    grad_down = contract_rows(hidden, cots_in)[None]
    grad_gate = contract_rows(tokens_in, d_gate)[None]
    grad_up = contract_rows(tokens_in, d_up)[None]
    extended = jnp.concatenate([d_conv_out, following], axis=0)
    taps = conv_taps.astype(f32)
    d_mixed = taps[2] * extended[:-2] + taps[1] * extended[1:-1] + taps[0] * extended[2:]
    grad_c = (d_mixed * conv_in.astype(f32)).astype(bf16)
    grad_conv_in = (d_mixed * c_gate.astype(f32)).astype(bf16)
    return (grad_gate, grad_up, grad_down, grad_out_weight, mid_grad, grad_b, grad_c, grad_conv_in)


def solution(mesh):
    placed = (
        P("sp", "tp"),
        P("sp", "tp"),
        P("tp"),
        P("sp", None),
        P("sp"),
        P("sp"),
        P("sp", None, "tp"),
        P("sp", None, "tp"),
        P("sp", "tp", None),
        P(None, "tp"),
        P("tp"),
        P("sp", "tp"),
        P("sp", "tp"),
        P("sp", "tp"),
        P("sp", "tp"),
        P(None, "tp"),
    )
    return jax.shard_map(
        shards,
        mesh=mesh,
        in_specs=placed,
        out_specs=(
            P("sp", None, "tp"),
            P("sp", None, "tp"),
            P("sp", "tp", None),
            P("sp", "tp"),
            P("sp", "tp"),
            P("sp", "tp"),
            P("sp", "tp"),
            P("sp", "tp"),
        ),
        check_vma=False,
    )
```

time: 233 us -> 203 us (0.87)
  Pallas kernels: 199 us -> 171 us
  other arithmetic: 7.79 us -> 3.57 us
  matrix products: 19.3 us -> 22.4 us
    pallas_call x1, Pallas kernels: 168 us -> 134 us  [experts(): pl.pallas_call(functools.partial(expert_kernel, dims), out_shape=(jax.Sha...]
    pallas_call x1, Pallas kernels: 31.4 us -> 37.3 us  [combine(): pl.pallas_call(functools.partial(combine_kernel, (A, B, rows, F)), out_sh...]
    dot_general x2, matrix products: 2.87 us -> 6.14 us  [group_mean(): jnp.dot(values, blocks, precision=lax.Precision.HIGHEST, preferred_elemen...]
  transfers between devices with their start and end apart: 1 -> 1, of which waited for: 0 -> 0; matrix products, arithmetic and copies ran while one was open for 6% -> 7% of each run, Pallas kernels for 13% -> 18%
where the time goes in v1:
time: 203 us; the launch traced here: 202 us
  Pallas kernels  171 us (84%)
  matrix products  22.4 us (11%)
  other arithmetic  3.57 us (2%)
  local copies, waits for them, and re-layouts  2.77 us (1%)
    pallas_call x1, Pallas kernels, experts(): pl.pallas_call(functools.partial(expert_kernel, dims), out_shape=(jax.Sha...  134 us
    pallas_call x1, Pallas kernels, combine(): pl.pallas_call(functools.partial(combine_kernel, (A, B, rows, F)), out_sh...  37.3 us
    dot_general x3, matrix products, contract_rows(): lax.dot_general(left, right, (((0,), (0,)), ((), ())), preferred_element_...  13.3 us
    dot_general x2, matrix products, group_mean(): jnp.dot(values, blocks, precision=lax.Precision.HIGHEST, preferred_elemen...  6.14 us
  transfers between devices with their start and end apart: 1, of which 0 were waited for; matrix products, arithmetic and copies ran while one was open for 7% of the time, Pallas kernels for 18%

profile of v1, /device:TPU:0, one launch (start us, length us, event | category | flops | bytes accessed | tf_op | source)
XLA Modules:
  0.0 202.3 jit_solution(9423745713891003756)
XLA Ops:
  0.6 0.7 convert_element_type.33
  1.3 2.8 %fusion.22 = f32[320,512]{1,0:T(8,128)} fusion(bf16[320,512]{1,0:T(8,128)(2,1)} %param.30, bf16[320,512]{1,0:T(8,128)(2,1)} %param.27, s32[512]{0:T(512)S(1)} %add_select_fusion), kind=kOutput, calls=%fused_computation.13 | convolution fusion | flops 1007878144 | bytes 1312768 | tf_op jit(solution)/shard_map/dot_general | solution.py:824
  4.1 134.1 %experts.1 = (bf16[320,1024]{1,0:T(8,128)(2,1)}, bf16[320,2048]{1,0:T(8,128)(2,1)}, bf16[1280,2048]{1,0:T(8,128)(2,1)}, bf16[1280,2048]{1,0:T(8,128)(2,1)}, bf16...) custom-call(bf16[320,1024]{1,0:T(8,128)(2,1)} %mid_in.1, bf16[320,1024]{1,0:T(8,128)(2,1)} %cot_in.1, ...), custom_call_target="tpu_custom_call" | custom-call | tf_op jit(solution)/shard_map/experts/pallas_call | solution.py:643
  138.2 0.0 copy-start.8
  138.3 0.0 copy-start.5
  138.3 3.0 %convolution_multiply_fusion = f32[320,512]{1,0:T(8,128)S(1)} fusion(bf16[320,2048]{1,0:T(8,128)(2,1)} %get-tuple-element.20.full, bf16[2048,512]{1,0:T(8,128)(2,1)} %param.25, f32[512]{0:T(512)S(1)} %convert_element_type.33), kind=kOutput, calls=%fused_computation.14 | convolution fusion | flops 671252480 | bytes 4065280 | tf_op jit(solution)/shard_map/dot_general | solution.py:883
  141.2 0.0 copy-done.8
  141.3 0.0 copy-start.7
  141.3 3.3 %convert_multiply_fusion.2 = (f32[320,512]{1,0:T(8,128)S(1)}, bf16[320,512]{1,0:T(8,128)(2,1)}, bf16[320,512]{1,0:T(8,128)(2,1)}) fusion(bf16[320,512]{1,0:T(8,128)(2,1)S(1)} %copy-done.8, bf16[320,512]{1,0:T(8,128)(2,1)} %param.30, f32[512]{0:T(512)S(1)} %convert_element_type.33, f32[320,512]{1,0:T(8,128)} %fusion.22, s32[512]{0:T(512)S(1)} %add_select_fusion, ...), kind=kOutput, calls=%fused_computation.18 | convolution fusion | flops 1010171904 | bytes 3280896 | tf_op jit(solution)/shard_map/dot_general | solution.py:824
  144.6 0.6 slice.26
  145.2 1.3 collective-permute-start
  146.5 0.0 copy-done.5
  146.5 0.0 copy-done.7
  146.5 0.0 copy-start.6
  146.5 0.0 slice-start
  146.5 4.5 %convolution_bitcast_fusion.2 = f32[1,2048,512]{2,1,0:T(8,128)} fusion(bf16[1280,2048]{1,0:T(8,128)(2,1)S(1)} %copy-done.5, bf16[1280,512]{1,0:T(8,128)(2,1)S(1)} %copy-done.7), kind=kOutput, calls=%fused_computation.2 | convolution fusion | flops 2684354560 | bytes 10747904 | tf_op jit(solution)/shard_map/dot_general | solution.py:33
  151.0 0.0 copy-done.6
  151.0 0.0 slice-start.1
  151.0 0.0 copy-start
  151.0 4.5 %convolution_bitcast_fusion.1 = f32[1,2048,512]{2,1,0:T(8,128)} fusion(bf16[1280,2048]{1,0:T(8,128)(2,1)S(1)} %copy-done.5, bf16[1280,512]{1,0:T(8,128)(2,1)S(1)} %copy-done.6), kind=kOutput, calls=%fused_computation.1 | convolution fusion | flops 2684354560 | bytes 10747904 | tf_op jit(solution)/shard_map/dot_general | solution.py:33
  155.5 0.0 slice-done
  155.5 0.0 slice-done.1
  155.5 0.0 copy-done
  155.5 0.0 copy-start.4
  155.5 4.4 %convolution_bitcast_fusion = f32[1,512,2048]{2,1,0:T(8,128)} fusion(bf16[1280,512]{1,0:T(8,128)(2,1)S(1)} %copy-done, bf16[1280,2048]{1,0:T(8,128)(2,1)S(1)} %bitcast.22), kind=kOutput, calls=%fused_computation | convolution fusion | flops 2684354560 | bytes 10747904 | tf_op jit(solution)/shard_map/dot_general | solution.py:33
  159.9 0.0 copy-done.4
  159.9 0.0 copy-start.3
  159.9 0.6 fusion.41
  160.5 37.3 %combine.1 = f32[128,512]{1,0:T(8,128)} custom-call(bf16[320,2048]{1,0:T(8,128)(2,1)} %get-tuple-element.20.full, bf16[320,512]{1,0:T(8,128)(2,1)} %get-tuple-element.26.normed), custom_call_target="tpu_custom_call" | custom-call | tf_op jit(solution)/shard_map/combine/pallas_call | solution.py:801
  197.8 0.0 copy-start.1
  197.8 0.0 copy-start.2
  197.9 0.0 collective-permute-done
  197.9 2.0 %multiply_convert_fusion = (bf16[320,512]{1,0:T(8,128)(2,1)}, f32[320,512]{1,0:T(8,128)S(1)}) fusion(bf16[320,512]{1,0:T(8,128)(2,1)} %param.28, f32[2,512]{1,0:T(2,128)} %collective-permute-done, f32[320,512]{1,0:T(8,128)S(1)} %get-tuple-element.24, f32[512]{0:T(512)} %bitcast.28, f32[512]{0:T(512)} %bitcast.27, f32[512]{0:T(512)} %bitcast.26), kind=kLoop, calls=%fused_computation.28 | loop fusion | flops 1638400 | bytes 1976320 | tf_op jit(solution)/shard_map/convert_element_type | solution.py:897
  199.9 0.0 copy-done.3
  199.9 0.8 multiply_convert_fusion.1
  200.8 0.0 copy-done.1
  200.8 0.7 copy.26
  201.5 0.0 copy-done.2
  201.5 0.8 copy.27
  (2 shorter events, 0.0 us)
Async XLA Ops:
  138.2 3.0 %copy-start.8 = (bf16[320,512]{1,0:T(8,128)(2,1)S(1)}, bf16[320,512]{1,0:T(8,128)(2,1)}, u32[]{:S(2)}) copy-start(bf16[320,512]{1,0:T(8,128)(2,1)} %param.27) | copy-start | bytes 983044
  138.3 8.2 %copy-start.5 = (bf16[1280,2048]{1,0:T(8,128)(2,1)S(1)}, bf16[1280,2048]{1,0:T(8,128)(2,1)}, u32[]{:S(2)}) copy-start(bf16[1280,2048]{1,0:T(8,128)(2,1)} %get-tuple-element.15) | copy-start | bytes 15728644
  141.3 5.3 %copy-start.7 = (bf16[1280,512]{1,0:T(8,128)(2,1)S(1)}, bf16[1280,512]{1,0:T(8,128)(2,1)}, u32[]{:S(2)}) copy-start(bf16[1280,512]{1,0:T(8,128)(2,1)} %get-tuple-element.16) | copy-start | bytes 3932164
  145.2 52.7 %collective-permute-start = (f32[2,512]{1,0:T(2,128)}, f32[2,512]{1,0:T(2,128)}, u32[]{:S(2)}, u32[]{:S(2)}) collective-permute-start(f32[2,512]{1,0:T(2,128)} %slice.26), channel_id=1, source_target_pairs={{2,0},{4,2},{6,4},{8,6},{10,8},{12,10},{14,12},{16,14},{18,16},{20... | collective-permute-start | bytes 12296 | tf_op jit(solution)/shard_map/ppermute | solution.py:24
  146.5 4.5 %copy-start.6 = (bf16[1280,512]{1,0:T(8,128)(2,1)S(1)}, bf16[1280,512]{1,0:T(8,128)(2,1)}, u32[]{:S(2)}) copy-start(bf16[1280,512]{1,0:T(8,128)(2,1)} %get-tuple-element.17) | copy-start | bytes 3932164
  146.5 8.9 %slice-start = ((s8[5242880]{0:T(1024)(128)(4,1)}), s8[4194304]{0:T(1024)(128)(4,1)S(1)}, s32[]{:S(2)}) async-start(s8[5242880]{0:T(1024)(128)(4,1)} %bitcast.21), calls=%async_computation | async-start | bytes 8388608
  151.0 4.5 %slice-start.1 = ((s8[5242880]{0:T(1024)(128)(4,1)}), s8[1048576]{0:T(1024)(128)(4,1)S(1)}, s32[]{:S(2)}) async-start(s8[5242880]{0:T(1024)(128)(4,1)} %bitcast.21), calls=%async_computation.1 | async-start | bytes 2097152
  151.0 4.5 %copy-start = (bf16[1280,512]{1,0:T(8,128)(2,1)S(1)}, bf16[1280,512]{1,0:T(8,128)(2,1)}, u32[]{:S(2)}) copy-start(bf16[1280,512]{1,0:T(8,128)(2,1)} %get-tuple-element.18) | copy-start | bytes 3932164
  155.5 4.4 %copy-start.4 = (bf16[3,512]{1,0:T(4,128)(2,1)S(1)}, bf16[3,512]{1,0:T(4,128)(2,1)}, u32[]{:S(2)}) copy-start(bf16[3,512]{1,0:T(4,128)(2,1)} %param.31) | copy-start | bytes 9220
  159.9 40.0 %copy-start.3 = (bf16[320,512]{1,0:T(8,128)(2,1)S(1)}, bf16[320,512]{1,0:T(8,128)(2,1)}, u32[]{:S(2)}) copy-start(bf16[320,512]{1,0:T(8,128)(2,1)} %param.29) | copy-start | bytes 983044
  197.8 2.9 %copy-start.1 = (f32[128,512]{1,0:T(8,128)S(1)}, f32[128,512]{1,0:T(8,128)}, u32[]{:S(2)}) copy-start(f32[128,512]{1,0:T(8,128)} %combine.1) | copy-start | bytes 786436
  197.8 3.6 %copy-start.2 = (bf16[320,1024]{1,0:T(8,128)(2,1)S(1)}, bf16[320,1024]{1,0:T(8,128)(2,1)}, u32[]{:S(2)}) copy-start(bf16[320,1024]{1,0:T(8,128)(2,1)} %get-tuple-element.42) | copy-start | bytes 1966084

commit v2 on v1

--- a/solution.py
+++ b/solution.py
@@ -16,12 +16,6 @@
 epsilon = 1e-06
 
 f32, bf16 = jnp.float32, jnp.bfloat16
-
-
-def from_behind(block, axis, distance):
-    devices = range(lax.axis_size(axis))
-    route = [(i - distance, i) for i in devices if i - distance in devices]
-    return lax.ppermute(block, axis, route)
 
 
 def silu_parts(pre):
@@ -706,32 +700,67 @@
     )(mid, cot, ids, prob, first, gain, gate, up, down)
 
 
-def combine_kernel(dims, full, normed, out, term, plane_in, line_out, line_in, p_send, p_recv, l_send, l_recv):
-    A, B, rows, F = dims
+def group_mean(values, blocks):
+    total = jnp.zeros(values.shape, f32)
+    for _ in range(3):
+        part = values.astype(bf16)
+        total = total + jnp.dot(part, blocks, preferred_element_type=f32)
+        values = values - part.astype(f32)
+    return total * (1.0 / GROUP)
+
+
+def mixer_kernel(
+    dims,
+    full_in, b_in, y_in, weight_in, c_in, x_in, cgain_in, taps_in,
+    grad_weight, grad_b, grad_c, grad_x,
+    full, b_gate, y, weight, c_gate, x, gated, rms, scaled, flow, normed,
+    term, plane_in, line_out, line_in,
+    ld, p_send, p_recv, l_send, l_recv, halo_sem,
+):
+    A, B, rows, R, F = dims
+    n = A * B
+    edge = 8
     me, c = lax.axis_index("sp"), lax.axis_index("tp")
     z, q = lax.div(me, B), lax.rem(me, B)
+    loads = [
+        pltpu.make_async_copy(src, dst, ld.at[k])
+        for k, (src, dst) in enumerate(
+            ((b_in, b_gate), (y_in, y), (full_in, full), (weight_in, weight), (c_in, c_gate), (x_in, x))
+        )
+    ]
+    for load in loads:
+        load.start()
     barrier = pltpu.get_barrier_semaphore()
+
+    def hello(peer):
+        pl.semaphore_signal(barrier, inc=1, device_id=(peer, c), device_id_type=MESH)
 
     @pl.loop(1, B)
     def _(k):
-        pl.semaphore_signal(
-            barrier, inc=1, device_id=(z * B + lax.rem(q + k, B), c), device_id_type=MESH
-        )
+        hello(z * B + lax.rem(q + k, B))
 
     @pl.loop(1, A)
     def _(j):
-        pl.semaphore_signal(
-            barrier, inc=1, device_id=(lax.rem(z + j, A) * B + q, c), device_id_type=MESH
-        )
-
-    def lot(x):
-        return pl.ds(pl.multiple_of(x * rows, rows), rows)
+        hello(lax.rem(z + j, A) * B + q)
+
+    apart_before = (q == 0) & (z > 0)
+    apart_after = (q == B - 1) & (z < A - 1)
+
+    @pl.when(apart_before)
+    def _():
+        hello(me - 1)
+
+    @pl.when(apart_after)
+    def _():
+        hello(me + 1)
+
+    def lot(k):
+        return pl.ds(pl.multiple_of(k * rows, rows), rows)
 
     def plane_send(s, k):
         peer = lax.rem(q + k, B)
         return remote(
-            term.at[s, lot(peer)], plane_in.at[s, k], p_send.at[s, k], p_recv.at[s, k],
-            (z * B + peer, c),
+            term.at[s, lot(peer)], plane_in.at[s, k], p_send.at[s], p_recv.at[s, k], (z * B + peer, c)
         )
 
     def line_send(s):
@@ -740,90 +769,145 @@
             (lax.rem(z + s, A) * B + q, c),
         )
 
-    def product(s):
-        block = cols_at(lax.rem(z + s, A) * (B * rows), B * rows)
-        got = contract_rows(full[:, block], normed[...])
-        term[s] = got.astype(bf16)
+    lane = lax.broadcasted_iota(jnp.int32, (F, F), 0) // GROUP
+    blocks = jnp.where(lane == lax.broadcasted_iota(jnp.int32, (F, F), 1) // GROUP, 1.0, 0.0)
+    blocks = blocks.astype(bf16)
+    cgain = cgain_in[...].astype(f32).reshape(1, F)
+    loads[0].wait()
+    loads[1].wait()
+    gated[...] = b_gate[...].astype(f32) * y[...].astype(f32)
+    rms[...] = lax.rsqrt(group_mean(gated[...] * gated[...], blocks) + epsilon)
+    normed[...] = (gated[...] * rms[...] * cgain).astype(bf16)
+    loads[2].wait()
 
     @pl.loop(0, A)
     def _(j):
         s = A - 1 - j
-        product(s)
+        block = cols_at(lax.rem(z + s, A) * (B * rows), B * rows)
+        term[s] = contract_rows(full[:, block], normed[...]).astype(bf16)
 
         @pl.when(j == 0)
         def _():
-            pl.semaphore_wait(barrier, A + B - 2)
+            pl.semaphore_wait(
+                barrier, A + B - 2 + jnp.where(apart_before, 1, 0) + jnp.where(apart_after, 1, 0)
+            )
 
         @pl.loop(1, B)
         def _(k):
             plane_send(s, k).start()
 
+    loads[3].wait()
+    scaled[...] = cgain * jnp.dot(full[...], weight[...], preferred_element_type=f32)
+    inner = group_mean(gated[...] * scaled[...], blocks)
+    d_gated = rms[...] * scaled[...] - gated[...] * (rms[...] * rms[...] * rms[...] * inner)
+    grad_b[...] = (d_gated * y[...].astype(f32)).astype(bf16)
+    flow[0:R, :] = d_gated * b_gate[...].astype(f32)
+    head, tail = flow.at[pl.ds(0, edge)], flow.at[pl.ds(R, edge)]
+    to_before = remote(head, tail, halo_sem.at[0], halo_sem.at[1], (me - 1, c))
+
+    @pl.when(me > 0)
+    def _():
+        to_before.start()
+
+    @pl.when(me == n - 1)
+    def _():
+        flow[R : R + edge, :] = jnp.zeros((edge, F), f32)
+
     def plane_sum(s):
-        out[...] = term[s, lot(q), :].astype(f32)
+        grad_weight[...] = term[s, lot(q), :].astype(f32)
 
         @pl.loop(1, B)
         def _(k):
             plane_send(s, k).wait_recv()
-            out[...] += plane_in[s, k].astype(f32)
+            grad_weight[...] += plane_in[s, k].astype(f32)
 
     @pl.loop(0, A - 1)
     def _(j):
         s = A - 1 - j
         plane_sum(s)
-        line_out[s] = out[...].astype(bf16)
+        line_out[s] = grad_weight[...].astype(bf16)
         line_send(s).start()
 
     plane_sum(0)
+    for load in loads[4:]:
+        load.wait()
+
+    @pl.when(me < n - 1)
+    def _():
+        remote(tail, tail, halo_sem.at[0], halo_sem.at[1], (me, 1 - c)).wait_recv()
+
+    taps = taps_in[...].astype(f32)
+    d_mixed = (
+        taps[2:3] * flow[0:R, :] + taps[1:2] * flow[1 : R + 1, :] + taps[0:1] * flow[2 : R + 2, :]
+    )
+    grad_c[...] = (d_mixed * x[...].astype(f32)).astype(bf16)
+    grad_x[...] = (d_mixed * c_gate[...].astype(f32)).astype(bf16)
 
     @pl.loop(1, A)
     def _(s):
         line_send(s).wait_recv()
-        out[...] += line_in[s].astype(f32)
+        grad_weight[...] += line_in[s].astype(f32)
+
+    @pl.when(me > 0)
+    def _():
+        to_before.wait_send()
 
     @pl.loop(0, A)
     def _(s):
-        @pl.loop(1, B)
-        def _(k):
-            plane_send(s, k).wait_send()
+        sent = plane_in.at[s, pl.ds(0, B - 1)]
+        remote(sent, sent, p_send.at[s], p_recv.at[s, 1], (me, 1 - c)).wait_send()
 
         @pl.when(s > 0)
         def _():
             line_send(s).wait_send()
 
 
-def combine(full, normed, n, plane, ident):
+def mixer(full, b_gate, y, weight, c_gate, x, cgain, taps, n, plane, ident):
     R, W = full.shape
-    F = normed.shape[1]
+    F = b_gate.shape[1]
     A, B = n // plane, plane
     rows = W // n
+    anywhere = pl.BlockSpec(memory_space=pl.ANY)
     vmem = pl.BlockSpec(memory_space=pltpu.VMEM)
     dma = pltpu.SemaphoreType.DMA
     return pl.pallas_call(
-        functools.partial(combine_kernel, (A, B, rows, F)),
-        out_shape=jax.ShapeDtypeStruct((rows, F), f32),
-        in_specs=[vmem, vmem],
-        out_specs=vmem,
+        functools.partial(mixer_kernel, (A, B, rows, R, F)),
+        out_shape=(
+            jax.ShapeDtypeStruct((rows, F), f32),
+            jax.ShapeDtypeStruct((R, F), bf16),
+            jax.ShapeDtypeStruct((R, F), bf16),
+            jax.ShapeDtypeStruct((R, F), bf16),
+        ),
+        in_specs=[anywhere] * 6 + [vmem] * 2,
+        out_specs=(vmem,) * 4,
         scratch_shapes=[
+            pltpu.VMEM((R, W), bf16),
+            pltpu.VMEM((R, F), bf16),
+            pltpu.VMEM((R, F), bf16),
+            pltpu.VMEM((W, F), bf16),
+            pltpu.VMEM((R, F), bf16),
+            pltpu.VMEM((R, F), bf16),
+            pltpu.VMEM((R, F), f32),
+            pltpu.VMEM((R, F), f32),
+            pltpu.VMEM((R, F), f32),
+            pltpu.VMEM((R + 8, F), f32),
+            pltpu.VMEM((R, F), bf16),
             pltpu.VMEM((A, B * rows, F), bf16),
             pltpu.VMEM((A, B, rows, F), bf16),
             pltpu.VMEM((A, rows, F), bf16),
             pltpu.VMEM((A, rows, F), bf16),
-            dma((A, B)),
+            dma((6,)),
+            dma((A,)),
             dma((A, B)),
             dma((A,)),
             dma((A,)),
+            dma((2,)),
         ],
         compiler_params=pltpu.CompilerParams(
             collective_id=ident, has_side_effects=True, vmem_limit_bytes=VMEM_LIMIT
         ),
-        name="combine",
-    )(full, normed)
-
-
-def group_mean(values, blocks):
-    return jnp.dot(
-        values, blocks, precision=lax.Precision.HIGHEST, preferred_element_type=jnp.float32
-    ) * (1.0 / GROUP)
+        name="mixer",
+    )(full, b_gate, y, weight, c_gate, x, cgain, taps)
 
 
 def shards(
@@ -868,33 +952,12 @@
         1,
     )
 
-    channel_count = b_gate.shape[1]
-    b32 = b_gate.astype(f32)
-    y32 = conv_out.astype(f32)
-    gated = b32 * y32
-    lane = jnp.arange(channel_count, dtype=jnp.int32) // GROUP
-    blocks = (lane[:, None] == lane[None, :]).astype(f32)
-    group_rms = lax.rsqrt(group_mean(gated * gated, blocks) + epsilon)
-    cgain = conv_gain.astype(f32)[None, :]
-    conv_normed = (gated * group_rms * cgain).astype(bf16)
-
-    grad_out_weight = combine(full_mid, conv_normed, n, plane, 2)
-
-    d_normed_conv = jnp.dot(full_mid, out_weight, preferred_element_type=f32)
-    g_dc = cgain * d_normed_conv
-    group_inner = group_mean(gated * g_dc, blocks)
-    d_gated = group_rms * g_dc - gated * (group_rms**3 * group_inner)
-    grad_b = (d_gated * y32).astype(bf16)
-    d_conv_out = d_gated * b32
-    following = from_behind(d_conv_out[:2], "sp", -1)
+    grad_out_weight, grad_b, grad_c, grad_conv_in = mixer(
+        full_mid, b_gate, conv_out, out_weight, c_gate, conv_in, conv_gain, conv_taps, n, plane, 2
+    )
     grad_down = contract_rows(hidden, cots_in)[None]
     grad_gate = contract_rows(tokens_in, d_gate)[None]
     grad_up = contract_rows(tokens_in, d_up)[None]
-    extended = jnp.concatenate([d_conv_out, following], axis=0)
-    taps = conv_taps.astype(f32)
-    d_mixed = taps[2] * extended[:-2] + taps[1] * extended[1:-1] + taps[0] * extended[2:]
-    grad_c = (d_mixed * conv_in.astype(f32)).astype(bf16)
-    grad_conv_in = (d_mixed * c_gate.astype(f32)).astype(bf16)
     return (grad_gate, grad_up, grad_down, grad_out_weight, mid_grad, grad_b, grad_c, grad_conv_in)
 
 

time: 203 us -> 191 us (0.941)
  matrix products: 22.4 us -> 16.8 us
  other arithmetic: 3.57 us -> 0.01 us
    dot_general x3 -> x0, matrix products: 9.11 us -> none  [the longest x2 6.14 us: group_mean(): jnp.dot(values, blocks, precision=lax.Precision.HIGHEST, preferred_elemen...]
    convert_element_type x3 -> x0, other arithmetic: 3.56 us -> none  [the longest x1 2.04 us: shards(): grad_conv_in = (d_mixed * c_gate.astype(f32)).astype(bf16)]
    dot_general x3, matrix products: 13.3 us -> 16.8 us  [contract_rows(): lax.dot_general(left, right, (((0,), (0,)), ((), ())), preferred_element_...]
    pallas_call x1, Pallas kernels: 37.3 us -> 34.9 us  [mixer(): pl.pallas_call(functools.partial(mixer_kernel, (A, B, rows, R, F)), out_s...]
    unnamed x24 -> x25, local copies, waits for them, and re-layouts: 1.59 us -> 3.75 us
  transfers between devices with their start and end apart: 1 -> 0, of which waited for: 0 -> 0; matrix products, arithmetic and copies ran while one was open for 7% -> 0% of each run, Pallas kernels for 18% -> 0%
where the time goes in v2:
time: 191 us; the launch traced here: 190 us
  Pallas kernels  169 us (88%)
  matrix products  16.8 us (9%)
  local copies, waits for them, and re-layouts  3.75 us (2%)
    pallas_call x1, Pallas kernels, experts(): pl.pallas_call(functools.partial(expert_kernel, dims), out_shape=(jax.Sha...  134 us
    pallas_call x1, Pallas kernels, mixer(): pl.pallas_call(functools.partial(mixer_kernel, (A, B, rows, R, F)), out_s...  34.9 us
    dot_general x3, matrix products, contract_rows(): lax.dot_general(left, right, (((0,), (0,)), ((), ())), preferred_element_...  16.8 us

profile of v2, /device:TPU:0, one launch (start us, length us, event | category | flops | bytes accessed | tf_op | source)
XLA Modules:
  0.0 190.4 jit_solution(7410968151359942447)
XLA Ops:
  0.6 134.1 %experts.1 = (bf16[320,1024]{1,0:T(8,128)(2,1)}, bf16[320,2048]{1,0:T(8,128)(2,1)}, bf16[1280,2048]{1,0:T(8,128)(2,1)}, bf16[1280,2048]{1,0:T(8,128)(2,1)}, bf16...) custom-call(bf16[320,1024]{1,0:T(8,128)(2,1)} %mid_in.1, bf16[320,1024]{1,0:T(8,128)(2,1)} %cot_in.1, ...), custom_call_target="tpu_custom_call" | custom-call | tf_op jit(solution)/shard_map/experts/pallas_call | solution.py:637
  134.8 34.9 %mixer.1 = (f32[128,512]{1,0:T(8,128)}, bf16[320,512]{1,0:T(8,128)(2,1)}, bf16[320,512]{1,0:T(8,128)(2,1)}, bf16[320,512]{1,0:T(8,128)(2,1)}) custom-call(bf16[320,2048]{1,0:T(8,128)(2,1)} %get-tuple-element.24.full_in, bf16[320,512]{1,0:T(8,128)(2,1)} %b_in.1, bf16[320,512]{1,0:T(8,128)(2,1)} %y_in.1, bf16[2048,512]{1,0:T(8,128)(2,1)} %weight_in.1, ...), custom_call_target="tpu_custom_call" | custom-call | tf_op jit(solution)/shard_map/mixer/pallas_call | solution.py:873
  169.7 0.0 copy-start.6
  169.7 0.0 copy-start.7
  169.7 0.0 slice-start
  169.7 8.0 %convolution_bitcast_fusion.2 = f32[1,2048,512]{2,1,0:T(8,128)} fusion(bf16[1280,2048]{1,0:T(8,128)(2,1)} %get-tuple-element.19, bf16[1280,512]{1,0:T(8,128)(2,1)} %get-tuple-element.20), kind=kOutput, calls=%fused_computation.2 | convolution fusion | flops 2684354560 | bytes 10747904 | tf_op jit(solution)/shard_map/dot_general | solution.py:27
  177.7 0.0 copy-done.6
  177.7 0.0 copy-done.7
  177.7 0.0 slice-start.1
  177.7 0.0 copy-start
  177.7 4.5 %convolution_bitcast_fusion.1 = f32[1,2048,512]{2,1,0:T(8,128)} fusion(bf16[1280,2048]{1,0:T(8,128)(2,1)S(1)} %copy-done.6, bf16[1280,512]{1,0:T(8,128)(2,1)S(1)} %copy-done.7), kind=kOutput, calls=%fused_computation.1 | convolution fusion | flops 2684354560 | bytes 10747904 | tf_op jit(solution)/shard_map/dot_general | solution.py:27
  182.2 0.0 slice-done
  182.2 0.0 slice-done.1
  182.2 0.0 copy-done
  182.2 0.0 copy-start.5
  182.2 0.0 copy-start.1
  182.2 0.0 copy-start.4
  182.2 0.0 copy-start.3
  182.2 0.0 copy-start.2
  182.2 4.4 %convolution_bitcast_fusion = f32[1,512,2048]{2,1,0:T(8,128)} fusion(bf16[1280,512]{1,0:T(8,128)(2,1)S(1)} %copy-done, bf16[1280,2048]{1,0:T(8,128)(2,1)S(1)} %bitcast.17), kind=kOutput, calls=%fused_computation | convolution fusion | flops 2684354560 | bytes 10747904 | tf_op jit(solution)/shard_map/dot_general | solution.py:27
  186.7 0.0 copy-done.5
  186.7 0.7 copy.29
  187.4 0.0 copy-done.1
  187.4 0.8 copy.30
  188.2 0.0 copy-done.4
  188.2 0.7 copy.31
  188.9 0.0 copy-done.3
  188.9 0.7 copy.32
  189.7 0.0 copy-done.2
  189.7 0.7 copy.33
  (1 shorter events, 0.0 us)
Async XLA Ops:
  169.7 8.0 %copy-start.6 = (bf16[1280,2048]{1,0:T(8,128)(2,1)S(1)}, bf16[1280,2048]{1,0:T(8,128)(2,1)}, u32[]{:S(2)}) copy-start(bf16[1280,2048]{1,0:T(8,128)(2,1)} %get-tuple-element.19) | copy-start | bytes 15728644
  169.7 8.0 %copy-start.7 = (bf16[1280,512]{1,0:T(8,128)(2,1)S(1)}, bf16[1280,512]{1,0:T(8,128)(2,1)}, u32[]{:S(2)}) copy-start(bf16[1280,512]{1,0:T(8,128)(2,1)} %get-tuple-element.21) | copy-start | bytes 3932164
  169.7 12.4 %slice-start = ((s8[5242880]{0:T(1024)(128)(4,1)}), s8[4194304]{0:T(1024)(128)(4,1)S(1)}, s32[]{:S(2)}) async-start(s8[5242880]{0:T(1024)(128)(4,1)} %bitcast.16), calls=%async_computation | async-start | bytes 8388608
  177.7 4.5 %slice-start.1 = ((s8[5242880]{0:T(1024)(128)(4,1)}), s8[1048576]{0:T(1024)(128)(4,1)S(1)}, s32[]{:S(2)}) async-start(s8[5242880]{0:T(1024)(128)(4,1)} %bitcast.16), calls=%async_computation.1 | async-start | bytes 2097152
  177.7 4.5 %copy-start = (bf16[1280,512]{1,0:T(8,128)(2,1)S(1)}, bf16[1280,512]{1,0:T(8,128)(2,1)}, u32[]{:S(2)}) copy-start(bf16[1280,512]{1,0:T(8,128)(2,1)} %get-tuple-element.22) | copy-start | bytes 3932164
  182.2 4.5 %copy-start.5 = (f32[128,512]{1,0:T(8,128)S(1)}, f32[128,512]{1,0:T(8,128)}, u32[]{:S(2)}) copy-start(f32[128,512]{1,0:T(8,128)} %get-tuple-element.41) | copy-start | bytes 786436
  182.2 5.2 %copy-start.1 = (bf16[320,1024]{1,0:T(8,128)(2,1)S(1)}, bf16[320,1024]{1,0:T(8,128)(2,1)}, u32[]{:S(2)}) copy-start(bf16[320,1024]{1,0:T(8,128)(2,1)} %get-tuple-element.42) | copy-start | bytes 1966084
  182.2 6.0 %copy-start.4 = (bf16[320,512]{1,0:T(8,128)(2,1)S(1)}, bf16[320,512]{1,0:T(8,128)(2,1)}, u32[]{:S(2)}) copy-start(bf16[320,512]{1,0:T(8,128)(2,1)} %get-tuple-element.43) | copy-start | bytes 983044
  182.2 6.7 %copy-start.3 = (bf16[320,512]{1,0:T(8,128)(2,1)S(1)}, bf16[320,512]{1,0:T(8,128)(2,1)}, u32[]{:S(2)}) copy-start(bf16[320,512]{1,0:T(8,128)(2,1)} %get-tuple-element.44) | copy-start | bytes 983044
  182.2 7.4 %copy-start.2 = (bf16[320,512]{1,0:T(8,128)(2,1)S(1)}, bf16[320,512]{1,0:T(8,128)(2,1)}, u32[]{:S(2)}) copy-start(bf16[320,512]{1,0:T(8,128)(2,1)} %get-tuple-element.45) | copy-start | bytes 983044

commit v3 on v2

--- a/solution.py
+++ b/solution.py
@@ -711,13 +711,16 @@
 
 def mixer_kernel(
     dims,
-    full_in, b_in, y_in, weight_in, c_in, x_in, cgain_in, taps_in,
-    grad_weight, grad_b, grad_c, grad_x,
+    full_in, b_in, y_in, weight_in, c_in, x_in, tokens_in, cots_in, hid_in, dgate_in, dup_in,
+    cgain_in, taps_in,
+    grad_weight, grad_b, grad_c, grad_x, grad_gate, grad_up, grad_down,
     full, b_gate, y, weight, c_gate, x, gated, rms, scaled, flow, normed,
-    term, plane_in, line_out, line_in,
-    ld, p_send, p_recv, l_send, l_recv, halo_sem,
+    term, plane_in, line_out, line_in, tokens, cots, hid, turned, slopes, wide_tile, down_tile,
+    ld, p_send, p_recv, l_send, l_recv, halo_sem, tile_sem,
 ):
     A, B, rows, R, F = dims
+    width = full.shape[1]
+    fills = width // COL
     n = A * B
     edge = 8
     me, c = lax.axis_index("sp"), lax.axis_index("tp")
@@ -725,7 +728,19 @@
     loads = [
         pltpu.make_async_copy(src, dst, ld.at[k])
         for k, (src, dst) in enumerate(
-            ((b_in, b_gate), (y_in, y), (full_in, full), (weight_in, weight), (c_in, c_gate), (x_in, x))
+            (
+                (b_in, b_gate),
+                (y_in, y),
+                (full_in, full),
+                (weight_in, weight),
+                (c_in, c_gate),
+                (x_in, x),
+                (hid_in, hid),
+                (tokens_in, tokens),
+                (dgate_in, slopes.at[:, pl.ds(0, F)]),
+                (dup_in, slopes.at[:, pl.ds(F, F)]),
+                (cots_in, cots),
+            )
         )
     ]
     for load in loads:
@@ -813,6 +828,37 @@
     def _():
         flow[R : R + edge, :] = jnp.zeros((edge, F), f32)
 
+    def tile_copies(u):
+        slot = lax.rem(u, 2)
+        at = cols_at(u * COL, COL)
+        return (
+            pltpu.make_async_copy(wide_tile.at[slot, :, pl.ds(0, F)], grad_gate.at[at], tile_sem.at[0, slot]),
+            pltpu.make_async_copy(wide_tile.at[slot, :, pl.ds(F, F)], grad_up.at[at], tile_sem.at[1, slot]),
+            pltpu.make_async_copy(down_tile.at[slot], grad_down.at[:, at], tile_sem.at[2, slot]),
+        )
+
+    def fill(u):
+        slot = lax.rem(u, 2)
+        at = cols_at(u * COL, COL)
+
+        @pl.when(u >= 2)
+        def _():
+            for copy in tile_copies(u - 2):
+                copy.wait()
+
+        wide_tile[slot] = contract_rows(tokens[:, at], slopes[...])
+        down_tile[slot] = jnp.dot(turned[...], cots[:, at], preferred_element_type=f32)
+        for copy in tile_copies(u):
+            copy.start()
+
+    per_sum = -(-fills // A)
+
+    def fill_after(j):
+        for k in range(per_sum):
+            @pl.when(j * per_sum + k < fills)
+            def _():
+                fill(j * per_sum + k)
+
     def plane_sum(s):
         grad_weight[...] = term[s, lot(q), :].astype(f32)
 
@@ -828,9 +874,16 @@
         line_out[s] = grad_weight[...].astype(bf16)
         line_send(s).start()
 
+        @pl.when(j == 0)
+        def _():
+            for load in loads[4:]:
+                load.wait()
+            turned[...] = hid[...].astype(f32).T.astype(bf16)
+
+        fill_after(j)
+
     plane_sum(0)
-    for load in loads[4:]:
-        load.wait()
+    fill_after(A - 1)
 
     @pl.when(me < n - 1)
     def _():
@@ -861,12 +914,17 @@
         def _():
             line_send(s).wait_send()
 
-
-def mixer(full, b_gate, y, weight, c_gate, x, cgain, taps, n, plane, ident):
+    for u in range(max(fills - 2, 0), fills):
+        for copy in tile_copies(u):
+            copy.wait()
+
+
+def mixer(full, b_gate, y, weight, c_gate, x, tokens, cots, hid, dgate, dup, cgain, taps, n, plane, ident):
     R, W = full.shape
     F = b_gate.shape[1]
     A, B = n // plane, plane
     rows = W // n
+    slots = tokens.shape[0]
     anywhere = pl.BlockSpec(memory_space=pl.ANY)
     vmem = pl.BlockSpec(memory_space=pltpu.VMEM)
     dma = pltpu.SemaphoreType.DMA
@@ -877,9 +935,12 @@
             jax.ShapeDtypeStruct((R, F), bf16),
             jax.ShapeDtypeStruct((R, F), bf16),
             jax.ShapeDtypeStruct((R, F), bf16),
+            jax.ShapeDtypeStruct((W, F), f32),
+            jax.ShapeDtypeStruct((W, F), f32),
+            jax.ShapeDtypeStruct((F, W), f32),
         ),
-        in_specs=[anywhere] * 6 + [vmem] * 2,
-        out_specs=(vmem,) * 4,
+        in_specs=[anywhere] * 11 + [vmem] * 2,
+        out_specs=(vmem,) * 4 + (anywhere,) * 3,
         scratch_shapes=[
             pltpu.VMEM((R, W), bf16),
             pltpu.VMEM((R, F), bf16),
@@ -896,18 +957,26 @@
             pltpu.VMEM((A, B, rows, F), bf16),
             pltpu.VMEM((A, rows, F), bf16),
             pltpu.VMEM((A, rows, F), bf16),
-            dma((6,)),
+            pltpu.VMEM((slots, W), bf16),
+            pltpu.VMEM((slots, W), bf16),
+            pltpu.VMEM((slots, F), bf16),
+            pltpu.VMEM((F, slots), bf16),
+            pltpu.VMEM((slots, 2 * F), bf16),
+            pltpu.VMEM((2, COL, 2 * F), f32),
+            pltpu.VMEM((2, F, COL), f32),
+            dma((11,)),
             dma((A,)),
             dma((A, B)),
             dma((A,)),
             dma((A,)),
             dma((2,)),
+            dma((3, 2)),
         ],
         compiler_params=pltpu.CompilerParams(
             collective_id=ident, has_side_effects=True, vmem_limit_bytes=VMEM_LIMIT
         ),
         name="mixer",
-    )(full, b_gate, y, weight, c_gate, x, cgain, taps)
+    )(full, b_gate, y, weight, c_gate, x, tokens, cots, hid, dgate, dup, cgain, taps)
 
 
 def shards(
@@ -952,12 +1021,25 @@
         1,
     )
 
-    grad_out_weight, grad_b, grad_c, grad_conv_in = mixer(
-        full_mid, b_gate, conv_out, out_weight, c_gate, conv_in, conv_gain, conv_taps, n, plane, 2
+    grad_out_weight, grad_b, grad_c, grad_conv_in, grad_gate, grad_up, grad_down = mixer(
+        full_mid,
+        b_gate,
+        conv_out,
+        out_weight,
+        c_gate,
+        conv_in,
+        tokens_in,
+        cots_in,
+        hidden,
+        d_gate,
+        d_up,
+        conv_gain,
+        conv_taps,
+        n,
+        plane,
+        2,
     )
-    grad_down = contract_rows(hidden, cots_in)[None]
-    grad_gate = contract_rows(tokens_in, d_gate)[None]
-    grad_up = contract_rows(tokens_in, d_up)[None]
+    grad_gate, grad_up, grad_down = grad_gate[None], grad_up[None], grad_down[None]
     return (grad_gate, grad_up, grad_down, grad_out_weight, mid_grad, grad_b, grad_c, grad_conv_in)
 
 

time: 191 us -> 188 us (0.984)
  matrix products: 16.8 us -> 0 us
  local copies, waits for them, and re-layouts: 3.75 us -> 14.3 us
  Pallas kernels: 169 us -> 172 us
    dot_general x3 -> x0, matrix products: 16.8 us -> none  [contract_rows(): lax.dot_general(left, right, (((0,), (0,)), ((), ())), preferred_element_...]
    unnamed x25 -> x22, local copies, waits for them, and re-layouts: 3.75 us -> 14.3 us
    pallas_call x1, Pallas kernels: 34.9 us -> 38.2 us  [mixer(): pl.pallas_call(functools.partial(mixer_kernel, (A, B, rows, R, F)), out_s...]
where the time goes in v3:
time: 188 us; the launch traced here: 187 us
  Pallas kernels  172 us (91%)
  local copies, waits for them, and re-layouts  14.3 us (8%)
    pallas_call x1, Pallas kernels, experts(): pl.pallas_call(functools.partial(expert_kernel, dims), out_shape=(jax.Sha...  134 us
    pallas_call x1, Pallas kernels, mixer(): pl.pallas_call(functools.partial(mixer_kernel, (A, B, rows, R, F)), out_s...  38.2 us
    unnamed x22, local copies, waits for them, and re-layouts  14.3 us

profile of v3, /device:TPU:0, one launch (start us, length us, event | category | flops | bytes accessed | tf_op | source)
XLA Modules:
  0.0 187.3 jit_solution(3515731634752989391)
XLA Ops:
  0.6 134.2 %experts.1 = (bf16[320,1024]{1,0:T(8,128)(2,1)}, bf16[320,2048]{1,0:T(8,128)(2,1)}, bf16[1280,2048]{1,0:T(8,128)(2,1)}, bf16[1280,2048]{1,0:T(8,128)(2,1)}, bf16...) custom-call(bf16[320,1024]{1,0:T(8,128)(2,1)} %mid_in.1, bf16[320,1024]{1,0:T(8,128)(2,1)} %cot_in.1, ...), custom_call_target="tpu_custom_call" | custom-call | tf_op jit(solution)/shard_map/experts/pallas_call | solution.py:637
  134.8 38.2 %mixer.1 = (f32[128,512]{1,0:T(8,128)}, bf16[320,512]{1,0:T(8,128)(2,1)}, bf16[320,512]{1,0:T(8,128)(2,1)}, bf16[320,512]{1,0:T(8,128)(2,1)}, f32[2048,512]{1,0:...) custom-call(bf16[320,2048]{1,0:T(8,128)(2,1)} %get-tuple-element.22.full_in, bf16[320,512]{1,0:T(8,128)(2,1)} %b_in.1, ...), custom_call_target="tpu_custom_call" | custom-call | tf_op jit(solution)/shard_map/mixer/pallas_call | solution.py:931
  173.0 0.0 copy-start.1
  173.0 4.8 %copy.32 = f32[1,2048,512]{2,1,0:T(8,128)} copy(f32[1,2048,512]{2,1,0:T(8,128)} %bitcast.9) | data formatting | bytes 8388608
  177.8 0.0 copy-done.1
  177.8 0.0 copy-start
  177.8 2.1 %copy.33 = f32[1,2048,512]{2,1,0:T(8,128)} copy(f32[1,2048,512]{2,1,0:T(8,128)S(1)} %bitcast.8) | data formatting | bytes 8388608
  179.9 1.6 copy-done
  181.5 0.0 copy-start.6
  181.5 0.0 copy-start.2
  181.5 0.0 copy-start.5
  181.5 0.0 copy-start.4
  181.5 0.0 copy-start.3
  181.5 2.1 %copy.34 = f32[1,512,2048]{2,1,0:T(8,128)} copy(f32[1,512,2048]{2,1,0:T(8,128)S(1)} %bitcast.7) | data formatting | bytes 8388608
  183.6 0.0 copy-done.6
  183.6 0.7 copy.35
  184.3 0.0 copy-done.2
  184.3 0.8 copy.36
  185.1 0.0 copy-done.5
  185.1 0.7 copy.37
  185.9 0.0 copy-done.4
  185.9 0.7 copy.38
  186.6 0.0 copy-done.3
  186.6 0.7 copy.39
Async XLA Ops:
  173.0 4.8 %copy-start.1 = (f32[2048,512]{1,0:T(8,128)S(1)}, f32[2048,512]{1,0:T(8,128)}, u32[]{:S(2)}) copy-start(f32[2048,512]{1,0:T(8,128)} %get-tuple-element.29) | copy-start | bytes 12582916
  177.8 3.7 %copy-start = (f32[512,2048]{1,0:T(8,128)S(1)}, f32[512,2048]{1,0:T(8,128)}, u32[]{:S(2)}) copy-start(f32[512,2048]{1,0:T(8,128)} %get-tuple-element.30) | copy-start | bytes 12582916
  181.5 2.1 %copy-start.6 = (f32[128,512]{1,0:T(8,128)S(1)}, f32[128,512]{1,0:T(8,128)}, u32[]{:S(2)}) copy-start(f32[128,512]{1,0:T(8,128)} %get-tuple-element.47) | copy-start | bytes 786436
  181.5 2.8 %copy-start.2 = (bf16[320,1024]{1,0:T(8,128)(2,1)S(1)}, bf16[320,1024]{1,0:T(8,128)(2,1)}, u32[]{:S(2)}) copy-start(bf16[320,1024]{1,0:T(8,128)(2,1)} %get-tuple-element.48) | copy-start | bytes 1966084
  181.5 3.6 %copy-start.5 = (bf16[320,512]{1,0:T(8,128)(2,1)S(1)}, bf16[320,512]{1,0:T(8,128)(2,1)}, u32[]{:S(2)}) copy-start(bf16[320,512]{1,0:T(8,128)(2,1)} %get-tuple-element.49) | copy-start | bytes 983044
  181.5 4.3 %copy-start.4 = (bf16[320,512]{1,0:T(8,128)(2,1)S(1)}, bf16[320,512]{1,0:T(8,128)(2,1)}, u32[]{:S(2)}) copy-start(bf16[320,512]{1,0:T(8,128)(2,1)} %get-tuple-element.50) | copy-start | bytes 983044
  181.5 5.1 %copy-start.3 = (bf16[320,512]{1,0:T(8,128)(2,1)S(1)}, bf16[320,512]{1,0:T(8,128)(2,1)}, u32[]{:S(2)}) copy-start(bf16[320,512]{1,0:T(8,128)(2,1)} %get-tuple-element.51) | copy-start | bytes 983044

commit v4 on v3

--- a/solution.py
+++ b/solution.py
@@ -11,7 +11,7 @@
 MESH = pl.DeviceIdType.MESH
 VMEM_LIMIT = 63 * 1024 * 1024
 COL = 256
-HALVES = 2
+HALVES = 4
 
 epsilon = 1e-06
 
@@ -494,7 +494,7 @@
             def _():
                 pick(1, h, b)
 
-    run_step = jnp.where(at_end, 0, HALVES - 1)
+    run_step = jnp.where(at_end, 1, HALVES - 1)
     lag = jnp.where(at_end, 1, 2)
 
     def step_of(u, before):
@@ -506,7 +506,7 @@
             take_in(0, z)
             run_forward(z)
 
-        @pl.when((r == 2) & (h == HALVES - 1 - run_step))
+        @pl.when((r == 2) & (h == jnp.where(at_end, HALVES - 1, 0)))
         def _():
             take_in(1, z)
             run_backward(z, -1)

time: 188 us -> 187 us (level)
  no operation moved by 1% of the time
where the time goes in v4:
time: 187 us
  Pallas kernels  172 us (92%)
  local copies, waits for them, and re-layouts  14.3 us (8%)
    pallas_call x1, Pallas kernels, experts(): pl.pallas_call(functools.partial(expert_kernel, dims), out_shape=(jax.Sha...  134 us
    pallas_call x1, Pallas kernels, mixer(): pl.pallas_call(functools.partial(mixer_kernel, (A, B, rows, R, F)), out_s...  38.2 us
    unnamed x22, local copies, waits for them, and re-layouts  14.3 us

profile of v4, /device:TPU:0, one launch (start us, length us, event | category | flops | bytes accessed | tf_op | source)
XLA Modules:
  0.0 187.1 jit_solution(1918175367716296601)
XLA Ops:
  0.6 133.9 %experts.1 = (bf16[320,1024]{1,0:T(8,128)(2,1)}, bf16[320,2048]{1,0:T(8,128)(2,1)}, bf16[1280,2048]{1,0:T(8,128)(2,1)}, bf16[1280,2048]{1,0:T(8,128)(2,1)}, bf16...) custom-call(bf16[320,1024]{1,0:T(8,128)(2,1)} %mid_in.1, bf16[320,1024]{1,0:T(8,128)(2,1)} %cot_in.1, ...), custom_call_target="tpu_custom_call" | custom-call | tf_op jit(solution)/shard_map/experts/pallas_call | solution.py:637
  134.5 38.2 %mixer.1 = (f32[128,512]{1,0:T(8,128)}, bf16[320,512]{1,0:T(8,128)(2,1)}, bf16[320,512]{1,0:T(8,128)(2,1)}, bf16[320,512]{1,0:T(8,128)(2,1)}, f32[2048,512]{1,0:...) custom-call(bf16[320,2048]{1,0:T(8,128)(2,1)} %get-tuple-element.22.full_in, bf16[320,512]{1,0:T(8,128)(2,1)} %b_in.1, ...), custom_call_target="tpu_custom_call" | custom-call | tf_op jit(solution)/shard_map/mixer/pallas_call | solution.py:931
  172.7 0.0 copy-start.1
  172.7 4.8 %copy.32 = f32[1,2048,512]{2,1,0:T(8,128)} copy(f32[1,2048,512]{2,1,0:T(8,128)} %bitcast.9) | data formatting | bytes 8388608
  177.5 0.0 copy-done.1
  177.6 0.0 copy-start
  177.6 2.1 %copy.33 = f32[1,2048,512]{2,1,0:T(8,128)} copy(f32[1,2048,512]{2,1,0:T(8,128)S(1)} %bitcast.8) | data formatting | bytes 8388608
  179.7 1.6 copy-done
  181.3 0.0 copy-start.6
  181.3 0.0 copy-start.2
  181.3 0.0 copy-start.5
  181.3 0.0 copy-start.4
  181.3 0.0 copy-start.3
  181.3 2.1 %copy.34 = f32[1,512,2048]{2,1,0:T(8,128)} copy(f32[1,512,2048]{2,1,0:T(8,128)S(1)} %bitcast.7) | data formatting | bytes 8388608
  183.3 0.0 copy-done.6
  183.3 0.7 copy.35
  184.0 0.0 copy-done.2
  184.0 0.8 copy.36
  184.9 0.0 copy-done.5
  184.9 0.7 copy.37
  185.6 0.0 copy-done.4
  185.6 0.7 copy.38
  186.3 0.0 copy-done.3
  186.3 0.7 copy.39
Async XLA Ops:
  172.7 4.8 %copy-start.1 = (f32[2048,512]{1,0:T(8,128)S(1)}, f32[2048,512]{1,0:T(8,128)}, u32[]{:S(2)}) copy-start(f32[2048,512]{1,0:T(8,128)} %get-tuple-element.29) | copy-start | bytes 12582916
  177.6 3.7 %copy-start = (f32[512,2048]{1,0:T(8,128)S(1)}, f32[512,2048]{1,0:T(8,128)}, u32[]{:S(2)}) copy-start(f32[512,2048]{1,0:T(8,128)} %get-tuple-element.30) | copy-start | bytes 12582916
  181.3 2.1 %copy-start.6 = (f32[128,512]{1,0:T(8,128)S(1)}, f32[128,512]{1,0:T(8,128)}, u32[]{:S(2)}) copy-start(f32[128,512]{1,0:T(8,128)} %get-tuple-element.47) | copy-start | bytes 786436
  181.3 2.8 %copy-start.2 = (bf16[320,1024]{1,0:T(8,128)(2,1)S(1)}, bf16[320,1024]{1,0:T(8,128)(2,1)}, u32[]{:S(2)}) copy-start(bf16[320,1024]{1,0:T(8,128)(2,1)} %get-tuple-element.48) | copy-start | bytes 1966084
  181.3 3.6 %copy-start.5 = (bf16[320,512]{1,0:T(8,128)(2,1)S(1)}, bf16[320,512]{1,0:T(8,128)(2,1)}, u32[]{:S(2)}) copy-start(bf16[320,512]{1,0:T(8,128)(2,1)} %get-tuple-element.49) | copy-start | bytes 983044
  181.3 4.3 %copy-start.4 = (bf16[320,512]{1,0:T(8,128)(2,1)S(1)}, bf16[320,512]{1,0:T(8,128)(2,1)}, u32[]{:S(2)}) copy-start(bf16[320,512]{1,0:T(8,128)(2,1)} %get-tuple-element.50) | copy-start | bytes 983044
  181.3 5.1 %copy-start.3 = (bf16[320,512]{1,0:T(8,128)(2,1)S(1)}, bf16[320,512]{1,0:T(8,128)(2,1)}, u32[]{:S(2)}) copy-start(bf16[320,512]{1,0:T(8,128)(2,1)} %get-tuple-element.51) | copy-start | bytes 983044
